TPU v7x, 512 devices: a whole 4x8x8 slice. The times are simulated.
512 devices in a mesh: fs: 128 (over z, y, core), tp: 4 (over x).
Axes of the slice: x: 4, y: 8, z: 8, core: 2. Of those that a mesh axis runs over, the one named last changes fastest.
Arguments:
- block_input: bfloat16 [24576, 2048], P('fs'), may hold values from -6 to 6
- query_cotangent: bfloat16 [24576, 1024], P('fs', 'tp'), may hold values from -0.0390625 to 0.0390625
- key_cotangent: bfloat16 [24576, 1024], P('fs', 'tp'), may hold values from -0.0390625 to 0.0390625
- query_factor: bfloat16 [2048, 256], P('fs'), may hold values from -0.125 to 0.125
- key_factor: bfloat16 [2048, 256], P('fs'), may hold values from -0.125 to 0.125
- query_first: float32 [256, 1024], P('fs', 'tp'), may hold values from -0.6 to 0.6
- query_second: float32 [256, 1024], P('fs', 'tp'), may hold values from 0.005 to 0.03
- key_first: float32 [256, 1024], P('fs', 'tp'), may hold values from -0.6 to 0.6
- key_second: float32 [256, 1024], P('fs', 'tp'), may hold values from 0.005 to 0.03
- query_weight: float32 [2048, 1024], P('fs', 'tp'), may hold values from -0.125 to 0.125
- key_weight: float32 [2048, 1024], P('fs', 'tp'), may hold values from -0.125 to 0.125
Outputs:
- query_update: float32 [2048, 1024], P('fs', 'tp')
- query_new: float32 [2048, 1024], P('fs', 'tp')
- query_copy: bfloat16 [2048, 1024], P(None, 'tp')
- query_first_new: float32 [256, 1024], P('fs', 'tp')
- query_second_new: float32 [256, 1024], P('fs', 'tp')
- key_update: float32 [2048, 1024], P('fs', 'tp')
- key_new: float32 [2048, 1024], P('fs', 'tp')
- key_copy: bfloat16 [2048, 1024], P(None, 'tp')
- key_first_new: float32 [256, 1024], P('fs', 'tp')
- key_second_new: float32 [256, 1024], P('fs', 'tp')
All inputs are finite; a program needn't handle non-finite values.
Results may differ from a plain program's by a relative error of at most 0.0005.
Values may be sent and summed in bfloat16 or wider, within the bound.
A program may use at most 64 MiB of HBM per device.

v0:
```python
import jax
import jax.numpy as jnp
from jax import lax
from jax.sharding import Mesh
from jax.sharding import PartitionSpec as P

FS = ("fs_0", "fs_1", "fs_2")


beta_one = 0.9
beta_two = 0.99
denom_floor = 0.001
scale_floor = 0.5
learn_rate = 0.02


def in_one_piece(arrays, axis, dim, along):
    widths = [a.shape[along] for a in arrays]
    both = jnp.concatenate(arrays, axis=along)
    whole = lax.all_gather(both, axis, axis=dim, tiled=True)
    return tuple(jnp.split(whole, [sum(widths[:k]) for k in range(1, len(widths))], axis=along))


def sum_in_order(tiles, axes, order):
    inside = tiles.shape[1:]
    tiles = tiles.reshape(*(lax.axis_size(a) for a in axes), *inside)
    tiles = jnp.moveaxis(tiles, order, range(len(axes))).reshape(-1, *inside)
    for k in order:
        tiles = lax.psum_scatter(tiles, axes[k], scatter_dimension=0, tiled=True)
    return tiles[0]


def split_up(x, dim, count):
    shape = x.shape
    tiles = x.reshape(*shape[:dim], count, shape[dim] // count, *shape[dim + 1 :])
    return jnp.moveaxis(tiles, dim, 0)


def scatter_axes(x, axes, order, dim):
    count = lax.axis_size(axes)
    return sum_in_order(split_up(x, dim, count), axes, order)


def sent_to_all(x, axis):
    count = lax.axis_size(axis)
    return lax.all_to_all(jnp.broadcast_to(x[None], (count, *x.shape)), axis, 0, 0, tiled=True)


def over_copies(x, axis):
    everything = sent_to_all(x, axis)
    return jnp.sum(everything, axis=0)


def packed_total(arrays, axis):
    ends = [0]
    for a in arrays:
        ends.append(ends[-1] + a.size)
    subtotal = over_copies(jnp.concatenate([a.ravel() for a in arrays]), axis)
    return tuple((subtotal[b:e].reshape(a.shape) for a, b, e in zip(arrays, ends, ends[1:])))


def moments(small, first, second):
    first_new = beta_one * first + (1.0 - beta_one) * small
    second_new = beta_two * second + (1.0 - beta_two) * small * small
    direction = first_new / (jnp.sqrt(second_new) + denom_floor)
    return (first_new, second_new, direction)


def split_three(values):
    upper = lax.optimization_barrier(values.astype(jnp.bfloat16))
    rest = values - upper.astype(jnp.float32)
    middle = lax.optimization_barrier(rest.astype(jnp.bfloat16))
    lower = (rest - middle.astype(jnp.float32)).astype(jnp.bfloat16)
    return (upper, middle, lower)


def project_tokens(mixed, cotangent):
    contract = (((0,), (0,)), ((), ()))
    total = jnp.zeros((mixed.shape[1], cotangent.shape[1]), jnp.float32)
    for piece in split_three(mixed):
        total = total + lax.dot_general(
            piece, cotangent, contract, preferred_element_type=jnp.float32
        )
    return total


def body(
    block_input,
    query_cotangent,
    key_cotangent,
    query_factor,
    key_factor,
    query_first,
    query_second,
    key_first,
    key_second,
    query_weight,
    key_weight,
):
    query_wide = query_factor.astype(jnp.float32)
    key_wide = key_factor.astype(jnp.float32)
    whole_query, whole_key = in_one_piece((query_factor, key_factor), FS, 0, 1)
    mixed_query = jnp.dot(block_input, whole_query, preferred_element_type=jnp.float32)
    mixed_key = jnp.dot(block_input, whole_key, preferred_element_type=jnp.float32)
    query_part = project_tokens(mixed_query, query_cotangent)
    key_part = project_tokens(mixed_key, key_cotangent)
    small_query, small_key = (
        scatter_axes(query_part, FS, (2, 0, 1), 0),
        scatter_axes(key_part, FS, (2, 0, 1), 0),
    )
    query_first_new, query_second_new, query_direction = moments(
        small_query, query_first, query_second
    )
    key_first_new, key_second_new, key_direction = moments(small_key, key_first, key_second)
    full_query, full_key = in_one_piece((query_direction, key_direction), FS, 0, 1)
    query_square, key_square = packed_total(
        (jnp.sum(full_query * full_query), jnp.sum(full_key * full_key)), "tp"
    )
    entry_count = full_query.shape[0] * full_query.shape[1] * lax.axis_size("tp")
    query_scale = 1.0 / jnp.maximum(jnp.sqrt(query_square / entry_count), scale_floor)
    key_scale = 1.0 / jnp.maximum(jnp.sqrt(key_square / entry_count), scale_floor)
    query_update = -query_scale * jnp.dot(query_wide, full_query, precision=lax.Precision.HIGHEST)
    key_update = -key_scale * jnp.dot(key_wide, full_key, precision=lax.Precision.HIGHEST)
    query_new = query_weight + learn_rate * query_update
    key_new = key_weight + learn_rate * key_update
    query_copy, key_copy = in_one_piece(
        (query_new.astype(jnp.bfloat16), key_new.astype(jnp.bfloat16)), FS, 0, 1
    )
    return (
        query_update,
        query_new,
        query_copy,
        query_first_new,
        query_second_new,
        key_update,
        key_new,
        key_copy,
        key_first_new,
        key_second_new,
    )


def solution(mesh):
    split = Mesh(mesh.devices.reshape(8, 8, 2, mesh.shape["tp"]), ("fs_0", "fs_1", "fs_2", "tp"))
    return jax.shard_map(
        body,
        mesh=split,
        in_specs=(
            P(FS, None),
            P(FS, "tp"),
            P(FS, "tp"),
            P(FS, None),
            P(FS, None),
            P(FS, "tp"),
            P(FS, "tp"),
            P(FS, "tp"),
            P(FS, "tp"),
            P(FS, "tp"),
            P(FS, "tp"),
        ),
        out_specs=(
            P(FS, "tp"),
            P(FS, "tp"),
            P(None, "tp"),
            P(FS, "tp"),
            P(FS, "tp"),
            P(FS, "tp"),
            P(FS, "tp"),
            P(None, "tp"),
            P(FS, "tp"),
            P(FS, "tp"),
        ),
        check_vma=False,
    )
```

profile of v0, /device:TPU:1, one launch (start us, length us, event | category | flops | bytes accessed | tf_op | source)
XLA Modules:
  0.0 408.6 jit_solution(5484928637678159431)
XLA Ops:
  7.2 0.0 copy-start
  7.2 0.0 all-gather.4.cloned.1.call-start
  7.2 1.4 pad_maximum_fusion
  8.6 0.0 all-gather.4.cloned.1.call-update
  8.6 0.0 all-reduce.14.cloned.1.call-start
  8.7 92.0 %all-gather.4.cloned.1.call-done = bf16[2048,512]{1,0:T(8,128)(2,1)} async-done(((bf16[16,512]{1,0:T(8,128)(2,1)}), bf16[2048,512]{1,0:T(8,128)(2,1)}) %all-gather.4.cloned.1.call-update) | async-done | bytes 2097168 | tf_op jit(solution)/shard_map/all_gather | solution.py:20
  100.7 1.7 fusion.17
  102.4 0.0 copy-start.1
  102.5 0.1 copy-done.11
  102.6 0.4 fusion.16
  103.0 0.3 copy-done.1
  103.4 0.2 fusion.19
  103.6 0.2 convolution_add_fusion.1
  103.8 0.2 convolution_add_fusion
  104.1 0.1 reshape_reshape.7
  104.2 0.8 copy.28
  105.0 0.2 fusion.18
  105.3 0.2 convolution_add_fusion.3
  105.5 0.2 convolution_add_fusion.2
  105.8 0.1 reshape_reshape.6
  105.9 0.8 copy.27
  106.7 0.0 all-reduce.14.cloned.1.call-update
  106.7 0.0 all-reduce.12.cloned.1.call-start
  106.8 1.3 dynamic-slice
  108.7 31.1 %all-reduce.14.cloned.1.call-done = (f32[128,2,256]{2,1,0:T(2,128)}, f32[128,2,256]{2,1,0:T(2,128)}) async-done(((f32[128,2,256]{2,1,0:T(2,128)}, f32[128,2,256]{2,1,0:T(2,128)}), (f32[128,2,256]{2,1,0:T(2,128)}, f32[128,2,256]{2,1,0:T(2,128)})) %all-reduce.14.cloned.1.call-update) | async-done | bytes 524304
  139.9 1.7 constant_dynamic-slice_fusion.1
  141.5 0.0 all-reduce.12.cloned.1.call-update
  141.6 0.0 all-gather.6.cloned.1.call-start
  141.6 1.3 dynamic-slice.4
  142.9 1.3 dynamic-slice.2
  144.8 72.2 %all-reduce.12.cloned.1.call-done = (f32[64,2,256]{2,1,0:T(2,128)}, f32[64,2,256]{2,1,0:T(2,128)}) async-done(((f32[64,2,256]{2,1,0:T(2,128)}, f32[64,2,256]{2,1,0:T(2,128)}), (f32[64,2,256]{2,1,0:T(2,128)}, f32[64,2,256]{2,1,0:T(2,128)})) %all-reduce.12.cloned.1.call-update) | async-done | bytes 262160
  217.0 0.7 constant_dynamic-slice_fusion
  217.7 0.7 constant_dynamic-slice_fusion.2
  218.5 22.6 %all-reduce.6 = (f32[8,2,256]{2,1,0:T(2,128)S(1)}, f32[8,2,256]{2,1,0:T(2,128)S(1)}) all-reduce(f32[8,2,256]{2,1,0:T(2,128)S(1)} %constant_dynamic-slice_fusion, f32[8,2,256]{2,1,0:T(2,128)S(1)} %constant_dynamic-slice_fusion.2), channel_id=7, replica_groups=mesh['fs_0'=8,'fs_1'=8,'fs_2'=2,'tp'=4] {'fs_1'}, use_global_device_ids=true, to_apply=%region_5.0.clone | all-reduce | flops 8192 | bytes 65536
  241.0 1.2 add_divide_fusion
  242.3 1.2 add_divide_fusion.1
  243.5 61.9 %all-gather = f32[128,2,512]{2,1,0:T(2,128)S(1)} all-gather(f32[1,2,512]{2,1,0:T(2,128)S(1)} %maximum_bitcast_fusion), channel_id=1, replica_groups=mesh['fs_0'=8,'fs_1'=8,'fs_2'=2,'tp'=4] {'fs_0','fs_1','fs_2'}, dimensions={0}, use_global_device_ids=true | all-gather | bytes 528384 | tf_op jit(solution)/shard_map/all_gather | solution.py:20
  305.4 0.4 reshape.61
  305.8 0.7 multiply_reduce_fusion.1
  306.5 1.4 pad_maximum_fusion.2
  307.9 7.9 %all_to_all.6 = f32[4,1,2]{2,1,0:T(1,128)S(1)} all-to-all(f32[4,1,2]{2,1,0:T(1,128)S(1)} %broadcast_in_dim.2), channel_id=1, replica_groups=mesh['fs_0'=8,'fs_1'=8,'fs_2'=2,'tp'=4] {'tp'}, dimensions={0} | all-to-all | bytes 64 | tf_op jit(solution)/shard_map/all_to_all | solution.py:46
  315.8 0.6 fusion.15
  317.8 0.8 fusion.11
  318.7 0.8 fusion.10
  319.5 0.6 pad_maximum_fusion.1
  320.1 0.0 all-gather.6.cloned.1.call-update
  320.1 79.0 %all-gather.6.cloned.1.call-done = bf16[2048,512]{1,0:T(8,128)(2,1)} async-done(((bf16[16,512]{1,0:T(8,128)(2,1)}), bf16[2048,512]{1,0:T(8,128)(2,1)}) %all-gather.6.cloned.1.call-update) | async-done | bytes 2097168 | tf_op jit(solution)/shard_map/all_gather | solution.py:20
  399.1 3.0 fusion.14
  (25 shorter events, 0.1 us)
Async XLA Ops:
  7.2 93.5 %copy-start = (bf16[192,2048]{1,0:T(8,128)(2,1)S(1)}, bf16[192,2048]{1,0:T(8,128)(2,1)}, u32[]{:S(2)}) copy-start(bf16[192,2048]{1,0:T(8,128)(2,1)} %param.11) | copy-start | bytes 2359300
  7.2 93.5 %all-gather.4.cloned.1.call-start = ((), (), s32[]{:S(2)}) async-start(), calls=%async_computation.1 | async-start | bytes 2113536 | tf_op jit(solution)/shard_map/all_gather | solution.py:20
  8.6 131.2 %all-reduce.14.cloned.1.call-start = ((), (), s32[]{:S(2)}) async-start(), calls=%async_computation.4 | async-start | bytes 1048576
  100.7 1.9 copy-start.11
  102.4 0.9 copy-start.1
  103.0 2.0 copy-start.2
  105.2 135.8 %copy-start.7 = (f32[2,256]{1,0:T(2,128)S(1)}, f32[2,256]{1,0:T(2,128)}, u32[]{:S(2)}) copy-start(f32[2,256]{1,0:T(2,128)} %param.19) | copy-start | bytes 6148
  105.2 135.8 %copy-start.8 = (f32[2,256]{1,0:T(2,128)S(1)}, f32[2,256]{1,0:T(2,128)}, u32[]{:S(2)}) copy-start(f32[2,256]{1,0:T(2,128)} %param.18) | copy-start | bytes 6148
  105.3 137.0 %copy-start.9 = (f32[2,256]{1,0:T(2,128)S(1)}, f32[2,256]{1,0:T(2,128)}, u32[]{:S(2)}) copy-start(f32[2,256]{1,0:T(2,128)} %param.17) | copy-start | bytes 6148
  105.3 137.0 %copy-start.10 = (f32[2,256]{1,0:T(2,128)S(1)}, f32[2,256]{1,0:T(2,128)}, u32[]{:S(2)}) copy-start(f32[2,256]{1,0:T(2,128)} %param.16) | copy-start | bytes 6148
  105.9 211.9 %copy-start.3 = (bf16[16,256]{1,0:T(8,128)(2,1)S(1)}, bf16[16,256]{1,0:T(8,128)(2,1)}, u32[]{:S(2)}) copy-start(bf16[16,256]{1,0:T(8,128)(2,1)} %param.15) | copy-start | bytes 24580
  105.9 211.9 %copy-start.5 = (f32[16,256]{1,0:T(8,128)S(1)}, f32[16,256]{1,0:T(8,128)}, u32[]{:S(2)}) copy-start(f32[16,256]{1,0:T(8,128)} %param.21) | copy-start | bytes 49156
  106.7 212.0 %copy-start.4 = (bf16[16,256]{1,0:T(8,128)(2,1)S(1)}, bf16[16,256]{1,0:T(8,128)(2,1)}, u32[]{:S(2)}) copy-start(bf16[16,256]{1,0:T(8,128)(2,1)} %param.14) | copy-start | bytes 24580
  106.7 212.0 %copy-start.6 = (f32[16,256]{1,0:T(8,128)S(1)}, f32[16,256]{1,0:T(8,128)}, u32[]{:S(2)}) copy-start(f32[16,256]{1,0:T(8,128)} %param.20) | copy-start | bytes 49156
  106.7 110.3 %all-reduce.12.cloned.1.call-start = ((), (), s32[]{:S(2)}) async-start(), calls=%async_computation.3 | async-start | bytes 524288
  141.6 257.5 %all-gather.6.cloned.1.call-start = ((), (), s32[]{:S(2)}) async-start(), calls=%async_computation.2 | async-start | bytes 2113536 | tf_op jit(solution)/shard_map/all_gather | solution.py:20
Sparse Core Ops, SparseCore 0:
  11.7 88.9 all-gather.3
  106.9 32.9 all-reduce.13
  142.8 74.1 all-reduce.11
  320.3 78.8 all-gather.5
where the time goes:
time: 409 us
  waiting for transfers between devices  274 us (67%)
  blocking collectives  92.4 us (23%)
  between operations  16.7 us (4%)
  local copies, waits for them, and re-layouts  13.2 us (3%)
  other arithmetic  6.57 us (2%)
  matrix products  5.15 us (1%)
    all_gather x2, waiting for transfers between devices, in_one_piece(): whole = lax.all_gather(both, axis, axis=dim, tiled=True)  171 us
    unnamed x6, waiting for transfers between devices  103 us
    all_gather x1, blocking collectives, in_one_piece(): whole = lax.all_gather(both, axis, axis=dim, tiled=True)  61.9 us
    unnamed x1, blocking collectives  22.6 us
  transfers between devices with their start and end apart: 4, of which 4 were waited for; matrix products, arithmetic and copies ran while one was open for 1% of the time, Pallas kernels for 0%

commit v1 on v0

v1 whole, which is shorter than its diff:
```python
import functools

import jax
import jax.numpy as jnp
from jax import lax
from jax.experimental import pallas as pl
from jax.experimental.pallas import tpu as pltpu
from jax.sharding import Mesh
from jax.sharding import PartitionSpec as P

MESH = pl.DeviceIdType.MESH
FS = ("z", "y", "c")
N = 8
SUBS = 4
FAR_FIRST = (4, 3, 5, 2, 6, 1, 7)
NEAR_FIRST = (1, 7, 2, 6, 3, 5, 4)

beta_one = 0.9
beta_two = 0.99
denom_floor = 0.001
scale_floor = 0.5
learn_rate = 0.02

f32 = jnp.float32
bf16 = jnp.bfloat16


def two_pieces(v):
    high = v.astype(bf16)
    low = (v - high.astype(f32)).astype(bf16)
    return high, low


class Part:
    def __init__(self, first, second, pos):
        self.first, self.second = first, second
        self.f, self.s, self.c = pos[first], pos[second], pos["c"]
        self.rows_second = second == "z"

    def block(self, buf, f, s, c):
        if self.rows_second:
            return buf.at[s, f // 2, f % 2, c]
        return buf.at[f // 2, f % 2, s, c]

    def sub(self, buf, j, s, c):
        if self.rows_second:
            return buf.at[s, j, :, c]
        return buf.at[j, :, s, c]

    def half(self, buf, h, s, c):
        if self.rows_second:
            return buf.at[s, pl.ds(2 * h, 2), :, c]
        return buf.at[pl.ds(2 * h, 2), :, s, c]

    def strip(self, buf, s, c):
        if self.rows_second:
            return buf.at[s, :, :, c]
        return buf.at[:, :, s, c]


def rows_of(buf, k, b):
    return (buf[b] if k == 0 else buf[b // 2, b % 2]).reshape(256, 256)


def own_rows(buf, k, z, y, c):
    return buf[z, y // 2, y % 2, c] if k == 0 else buf[z // 2, z % 2, y, c]


def ring(v, d):
    return lax.rem(v + (d + 2 * N), N)


class Sends:
    def __init__(self, sems):
        self.sems, self.used, self.open = sems, 0, []

    def __call__(self, src, dst, recv, to):
        copy = pltpu.make_async_remote_copy(
            src_ref=src,
            dst_ref=dst,
            send_sem=self.sems.at[self.used],
            recv_sem=recv,
            device_id=to,
            device_id_type=MESH,
        )
        self.used += 1
        copy.start()
        self.open.append(copy)

    def arrived(self, ref, recv, to):
        pltpu.make_async_remote_copy(
            src_ref=ref, dst_ref=ref, send_sem=self.sems.at[0], recv_sem=recv, device_id=to, device_id_type=MESH
        ).wait_recv()

    def finish(self):
        for copy in self.open:
            copy.wait_send()


def exchange_kernel(
    x_hbm, cq_hbm, ck_hbm, fq_hbm, fk_hbm, q1_hbm, q2_hbm, k1_hbm, k2_hbm, wq_hbm, wk_hbm,
    FQ, FK, WQ, WK, DQ, DK, total_ref, mom_ref,
    xv, cqv, ckv, fown, MQ, MK, MF, PB, PR, SB, R1, S1, R2, SS, T, M8,
    loc, send_sems, d1, rr, rl, dd, w1, wr, wl, wd, ms, ps, b1, b2, c1, cd, xs,
):
    pos = {a: lax.axis_index(a) for a in ("z", "y", "c")}
    me_x = lax.axis_index("tp")
    z, y, c = pos["z"], pos["y"], pos["c"]
    query, key = Part("y", "z", pos), Part("z", "y", pos)
    parts = (query, key)
    F, W, Dn, Mo = (FQ, FK), (WQ, WK), (DQ, DK), (MQ, MK)
    other = {"c": 1 - c}

    loads = []

    def load(src, dst):
        copy = pltpu.make_async_copy(src, dst, loc.at[len(loads)])
        copy.start()
        loads.append(copy)

    load(fq_hbm, fown.at[0])
    load(fk_hbm, fown.at[1])
    load(q1_hbm, MQ.at[z, 0])
    load(q2_hbm, MQ.at[z, 1])
    load(k1_hbm, MK.at[y, 0])
    load(k2_hbm, MK.at[y, 1])
    load(wq_hbm, query.block(WQ, query.f, query.s, c))
    load(wk_hbm, key.block(WK, key.f, key.s, c))
    load(cq_hbm, cqv)
    load(ck_hbm, ckv)
    load(x_hbm, xv)

    barrier = pltpu.get_barrier_semaphore()
    for d in range(1, N):
        pl.semaphore_signal(barrier, inc=1, device_id={"y": ring(y, d)}, device_id_type=MESH)
        pl.semaphore_signal(barrier, inc=1, device_id={"z": ring(z, d)}, device_id_type=MESH)
    pl.semaphore_signal(barrier, inc=1, device_id=other, device_id_type=MESH)
    for d in range(1, 4):
        pl.semaphore_signal(barrier, inc=1, device_id={"tp": lax.rem(me_x + d, 4)}, device_id_type=MESH)

    rank = lax.broadcasted_iota(jnp.int32, (256, 256), 0)
    slot = lax.broadcasted_iota(jnp.int32, (256, 256), 1)
    sf, sc, ss, si = slot >> 5, (slot >> 4) & 1, (slot >> 1) & 7, slot & 1
    places = (((ss * 8 + sf) * 2 + sc) * 2 + si, ((sf * 8 + ss) * 2 + sc) * 2 + si)
    loads[0].wait()
    loads[1].wait()
    for k, part in enumerate(parts):
        order = jnp.where(rank == places[k], 1.0, 0.0).astype(bf16)
        mine = jnp.dot(fown[k], order, preferred_element_type=f32).astype(bf16)
        part.block(F[k], part.f, part.s, c)[...] = mine

    for copy in loads[2:8]:
        copy.wait()
    pl.semaphore_wait(barrier, 2 * (N - 1) + 1 + 3)

    send = Sends(send_sems)

    def direct(k, buf, sems):
        part = parts[k]
        for d in FAR_FIRST:
            mine = part.block(buf, part.f, part.s, c)
            send(mine, mine, sems.at[k, d], {part.first: ring(part.f, d)})

    for k in (0, 1):
        direct(k, F[k], d1)

    def piece(k, t):
        return lax.rem(parts[k].f // 2 + t, SUBS)

    for t in range(4):
        for n in range(SUBS):
            for k, part in enumerate(parts):
                j = piece(k, n)
                right, left = {part.second: ring(part.s, 1)}, {part.second: ring(part.s, -1)}
                if t == 0:
                    for r in (0, 1):
                        fr = 2 * j + r
                        far = lax.rem(part.f - fr + N, N)

                        @pl.when(far != 0)
                        def _():
                            send.arrived(part.block(F[k], fr, part.s, c), d1.at[k, far], other)

                    mine = part.sub(F[k], j, part.s, c)
                    send(mine, mine, rr.at[k, 0, n], right)
                    send(mine, mine, rl.at[k, 0, n], left)
                else:
                    from_left = part.sub(F[k], j, ring(part.s, -t), c)
                    send.arrived(from_left, rr.at[k, t - 1, n], other)
                    if t < 3 or n < SUBS // 2:
                        send(from_left, from_left, rr.at[k, t, n], right)
                    from_right = part.sub(F[k], j, ring(part.s, t), c)
                    send.arrived(from_right, rl.at[k, t - 1, n], other)
                    if t < 3 or n >= SUBS // 2:
                        send(from_right, from_right, rl.at[k, t, n], left)
        for k, part in enumerate(parts):
            for s in [0] if t == 0 else [-t, t]:
                strip = part.strip(F[k], ring(part.s, s), c)
                send(strip, strip, dd.at[k, s + 3], other)
    for k, part in enumerate(parts):
        for n in range(SUBS):
            sems = rr if n < SUBS // 2 else rl
            send.arrived(part.sub(F[k], piece(k, n), ring(part.s, 4), c), sems.at[k, 3, n], other)
        strip = part.strip(F[k], ring(part.s, 4), c)
        send(strip, strip, dd.at[k, 7], other)

    for k, part in enumerate(parts):
        for d in FAR_FIRST:
            mine = Mo[k].at[part.s]
            send(mine, mine, ms.at[k, d], {part.second: ring(part.s, d)})
    for k in (0, 1):
        direct(k, W[k], w1)

    def weights_step(t):
        for k, part in enumerate(parts):
            right, left = {part.second: ring(part.s, 1)}, {part.second: ring(part.s, -1)}
            if t == 0:
                for d in NEAR_FIRST:
                    send.arrived(part.block(W[k], ring(part.f, -d), part.s, c), w1.at[k, d], other)
                mine = part.strip(W[k], part.s, c)
                send(mine, mine, wr.at[k, 0], right)
                send(mine, mine, wl.at[k, 0], left)
                send(mine, mine, wd.at[k, 3], other)
                continue
            if t < 4:
                from_left = part.strip(W[k], ring(part.s, -t), c)
                send.arrived(from_left, wr.at[k, t - 1], other)
                from_right = part.strip(W[k], ring(part.s, t), c)
                send.arrived(from_right, wl.at[k, t - 1], other)
                if t < 3:
                    send(from_left, from_left, wr.at[k, t], right)
                    send(from_right, from_right, wl.at[k, t], left)
                else:
                    low = part.half(W[k], 0, ring(part.s, -3), c)
                    send(low, low, wr.at[k, 3], right)
                    high = part.half(W[k], 1, ring(part.s, 3), c)
                    send(high, high, wl.at[k, 3], left)
                send(from_left, from_left, wd.at[k, 3 - t], other)
                send(from_right, from_right, wd.at[k, 3 + t], other)
                continue
            send.arrived(part.half(W[k], 0, ring(part.s, 4), c), wr.at[k, 3], other)
            send.arrived(part.half(W[k], 1, ring(part.s, 4), c), wl.at[k, 3], other)
            last = part.strip(W[k], ring(part.s, 4), c)
            send(last, last, wd.at[k, 7], other)

    for copy in loads[8:]:
        copy.wait()
    for k, part in enumerate(parts):
        for s in (0, -1, 1, -2, 2, -3, 3, 4):
            send.arrived(
                part.strip(F[k], ring(part.s, s), 1 - c), dd.at[k, s + 3], other
            )
        mixed = jnp.zeros((192, 256), f32)
        for b in range(N):
            block = rows_of(F[k], k, b)
            mixed += jnp.dot(xv[:, b * 256 : (b + 1) * 256], block, preferred_element_type=f32)
        cot = (cqv, ckv)[k][...]
        high, low = two_pieces(mixed)
        product = jnp.dot(high.T, cot, preferred_element_type=f32)
        product += jnp.dot(low.T, cot, preferred_element_type=f32)
        PB[k] = product.reshape(N, 2, 16, 256)
        half = PB.at[k, :, 1 - c]
        send(half, PR.at[k], ps.at[k], other)
    weights_step(0)

    for k, part in enumerate(parts):
        send.arrived(PR.at[k], ps.at[k], other)
        SB[k] = PB[k, :, c] + PR[k]
        for d in FAR_FIRST:
            to = ring(part.f, d)
            send(SB.at[k, to], R1.at[k, part.f], b1.at[k, d], {part.first: to})
    weights_step(1)
    for k, part in enumerate(parts):
        acc = SB[k, part.f]
        for d in NEAR_FIRST:
            src = ring(part.f, -d)
            send.arrived(R1.at[k, src], b1.at[k, d], other)
            acc += R1[k, src]
        R2[k, part.s] = acc
        for d in FAR_FIRST:
            mine = R2.at[k, part.s]
            send(mine, mine, b2.at[k, d], {part.second: ring(part.s, d)})
    for k, part in enumerate(parts):
        for d in NEAR_FIRST:
            src = ring(part.s, -d)
            send.arrived(Mo[k].at[src], ms.at[k, d], other)
        for b in range(N):
            for m in (0, 1):
                MF[k, m, 2 * b : 2 * b + 2, :] = Mo[k][b, m]
    weights_step(2)

    for k, part in enumerate(parts):
        for d in NEAR_FIRST:
            send.arrived(R2.at[k, ring(part.s, -d)], b2.at[k, d], other)
        small = R2[k, 0]
        for b in range(1, N):
            small += R2[k, b]
        first_new = beta_one * MF[k, 0] + (1.0 - beta_one) * small
        second_new = beta_two * MF[k, 1] + (1.0 - beta_two) * small * small
        Dn[k][part.f, c] = first_new / (jnp.sqrt(second_new) + denom_floor)
        for d in FAR_FIRST:
            mine = Dn[k].at[part.f, c]
            send(mine, mine, c1.at[k, d], {part.first: ring(part.f, d)})
        T[k, 0] = first_new
        T[k, 1] = second_new
    weights_step(3)
    for k, part in enumerate(parts):
        for m in (0, 1):
            for b in range(N):
                M8[k, m, b] = T[k, m, 2 * b : 2 * b + 2, :]
            mom_ref[k, m] = M8[k, m, part.s]
    for k, part in enumerate(parts):
        for d in NEAR_FIRST:
            send.arrived(Dn[k].at[ring(part.f, -d), c], c1.at[k, d], other)
        mine = Dn[k].at[:, c]
        send(mine, mine, cd.at[k], other)
    weights_step(4)
    sums = []
    for k, part in enumerate(parts):
        send.arrived(Dn[k].at[:, 1 - c], cd.at[k], other)
        full = Dn[k][...].reshape(256, 256)
        sums.append(jnp.sum(full * full, axis=(0, 1), keepdims=True))
    row = lax.broadcasted_iota(jnp.int32, (8, 256), 0)
    SS[me_x] = jnp.where(row == 0, sums[0], sums[1])
    for d in range(1, 4):
        mine = SS.at[me_x]
        send(mine, mine, xs.at[d], {"tp": lax.rem(me_x + d, 4)})
    for k, part in enumerate(parts):
        for s in (0, -1, 1, -2, 2, -3, 3, 4):
            send.arrived(part.strip(W[k], ring(part.s, s), 1 - c), wd.at[k, s + 3], other)
    for d in range(1, 4):
        send.arrived(SS.at[lax.rem(me_x + 4 - d, 4)], xs.at[d], other)
    total_ref[...] = ((SS[0] + SS[1]) + SS[2]) + SS[3]
    send.finish()


def update_kernel(
    FQ, FK, WQ, WK, DQ, DK, total_ref, mom_ref,
    uq_out, nq_out, cq_out, f1q_out, f2q_out, uk_out, nk_out, ck_out, f1k_out, f2k_out,
    copies, own, mom, sems, small_sems,
):
    z, y, c = (lax.axis_index(a) for a in FS)
    F, W, Dn = (FQ, FK), (WQ, WK), (DQ, DK)
    outs = ((uq_out, nq_out, cq_out, f1q_out, f2q_out), (uk_out, nk_out, ck_out, f1k_out, f2k_out))
    flight = []
    mom[...] = mom_ref[...]
    for k in (0, 1):
        for m in (0, 1):
            copy = pltpu.make_async_copy(mom.at[k, m], outs[k][3 + m], small_sems.at[k, m])
            copy.start()
            flight.append(copy)
    for k in (0, 1):
        total = total_ref[k : k + 1, :]
        scale = 1.0 / jnp.maximum(jnp.sqrt(total * (1.0 / 262144.0)), scale_floor)
        high, low = two_pieces(Dn[k][...].reshape(256, 256))

        def update_of(rows):
            whole = jnp.dot(rows, high, preferred_element_type=f32) + jnp.dot(rows, low, preferred_element_type=f32)
            return -scale * whole

        for b in range(N):
            update = update_of(rows_of(F[k], k, b))
            new = rows_of(W[k], k, b) + learn_rate * update
            copies[k, b] = new.astype(bf16)
            copy = pltpu.make_async_copy(copies.at[k, b], outs[k][2].at[pl.ds(b * 256, 256), :], sems.at[k, b])
            copy.start()
            flight.append(copy)
        update = update_of(own_rows(F[k], k, z, y, c))
        own[k, 0] = update
        own[k, 1] = own_rows(W[k], k, z, y, c) + learn_rate * update
        for m in (0, 1):
            copy = pltpu.make_async_copy(own.at[k, m], outs[k][m], small_sems.at[k, 2 + m])
            copy.start()
            flight.append(copy)
    for copy in flight:
        copy.wait()


def body(block_input, query_cotangent, key_cotangent, query_factor, key_factor,
         query_first, query_second, key_first, key_second, query_weight, key_weight):
    any_spec = pl.BlockSpec(memory_space=pl.ANY)
    vmem = pl.BlockSpec(memory_space=pltpu.VMEM)
    shape = jax.ShapeDtypeStruct
    by_z, by_y = (8, 4, 2, 2, 16, 256), (4, 2, 8, 2, 16, 256)
    dma = pltpu.SemaphoreType.DMA
    mid = pl.pallas_call(
        exchange_kernel,
        out_shape=(
            pltpu.VMEM(by_z, bf16), pltpu.VMEM(by_y, bf16), pltpu.VMEM(by_z, f32), pltpu.VMEM(by_y, f32),
            pltpu.VMEM((8, 2, 16, 256), f32), pltpu.VMEM((8, 2, 16, 256), f32),
            pltpu.VMEM((8, 256), f32), pltpu.VMEM((2, 2, 2, 256), f32),
        ),
        in_specs=[any_spec] * 11,
        out_specs=(vmem,) * 8,
        scratch_shapes=[
            pltpu.VMEM((192, 2048), bf16), pltpu.VMEM((192, 256), bf16), pltpu.VMEM((192, 256), bf16),
            pltpu.VMEM((2, 16, 256), bf16),
            pltpu.VMEM((8, 2, 2, 256), f32), pltpu.VMEM((8, 2, 2, 256), f32), pltpu.VMEM((2, 2, 16, 256), f32),
            pltpu.VMEM((2, 8, 2, 16, 256), f32), pltpu.VMEM((2, 8, 16, 256), f32), pltpu.VMEM((2, 8, 16, 256), f32),
            pltpu.VMEM((2, 8, 16, 256), f32), pltpu.VMEM((8, 256), f32), pltpu.VMEM((2, 8, 16, 256), f32),
            pltpu.VMEM((4, 8, 256), f32), pltpu.VMEM((2, 2, 16, 256), f32), pltpu.VMEM((2, 2, 8, 2, 256), f32),
            dma((11,)), dma((220,)),
            dma((2, 8)), dma((2, 4, 4)), dma((2, 4, 4)), dma((2, 8)),
            dma((2, 8)), dma((2, 4)), dma((2, 4)), dma((2, 8)),
            dma((2, 8)), dma((2,)), dma((2, 8)), dma((2, 8)), dma((2, 8)), dma((2,)), dma((4,)),
        ],
        compiler_params=pltpu.CompilerParams(collective_id=0, has_side_effects=True, vmem_limit_bytes=40 * 1024 * 1024),
    )(block_input, query_cotangent, key_cotangent, query_factor, key_factor,
      query_first, query_second, key_first, key_second, query_weight, key_weight)
    one = (
        shape((16, 256), f32), shape((16, 256), f32), shape((2048, 256), bf16), shape((2, 256), f32), shape((2, 256), f32),
    )
    return pl.pallas_call(
        update_kernel,
        out_shape=one + one,
        in_specs=[vmem] * 8,
        out_specs=(any_spec,) * 10,
        scratch_shapes=[
            pltpu.VMEM((2, 8, 256, 256), bf16), pltpu.VMEM((2, 2, 16, 256), f32), pltpu.VMEM((2, 2, 2, 256), f32),
            dma((2, 8)), dma((2, 4)),
        ],
        compiler_params=pltpu.CompilerParams(vmem_limit_bytes=40 * 1024 * 1024),
    )(*mid)


def solution(mesh):
    split = Mesh(mesh.devices.reshape(8, 8, 2, mesh.shape["tp"]), ("z", "y", "c", "tp"))
    rows, both = P(FS, None), P(FS, "tp")
    one = (both, both, P(None, "tp"), both, both)
    return jax.shard_map(
        body,
        mesh=split,
        in_specs=(rows, both, both, rows, rows, both, both, both, both, both, both),
        out_specs=one + one,
        check_vma=False,
    )
```

time: 409 us -> 82.7 us (0.20)
  waiting for transfers between devices: 274 us -> 0 us
  blocking collectives: 92.4 us -> 0 us
  Pallas kernels: 0 us -> 72.4 us
  between operations: 16.7 us -> 0.67 us
  other arithmetic: 6.57 us -> 0 us
  matrix products: 5.15 us -> 0 us
  local copies, waits for them, and re-layouts: 13.2 us -> 8.46 us
    all_gather x2 -> x0, waiting for transfers between devices: 171 us -> none  [in_one_piece(): whole = lax.all_gather(both, axis, axis=dim, tiled=True)]
    unnamed x6 -> x0, waiting for transfers between devices: 103 us -> none
    pallas_call x0 -> x2, Pallas kernels: none -> 72.4 us  [the longest x1 70.2 us: body(): pl.pallas_call(exchange_kernel, out_shape=(pltpu.VMEM(by_z, bf16), pltpu....]
    all_gather x1 -> x0, blocking collectives: 61.9 us -> none  [in_one_piece(): whole = lax.all_gather(both, axis, axis=dim, tiled=True)]
    unnamed x1 -> x0, blocking collectives: 22.6 us -> none
    all_to_all x1 -> x0, blocking collectives: 7.89 us -> none  [sent_to_all(): lax.all_to_all(jnp.broadcast_to(x[None], (count, *x.shape)), axis, 0, 0,...]
    dot_general x10 -> x0, matrix products: 5.15 us -> none  [the longest x1 1.75 us: body(): jnp.dot(block_input, whole_query, preferred_element_type=jnp.float32)]
    unnamed x31 -> x22, local copies, waits for them, and re-layouts: 7.82 us -> 8.46 us
  transfers between devices with their start and end apart: 4 -> 0, of which waited for: 4 -> 0; matrix products, arithmetic and copies ran while one was open for 1% -> 0% of each run, Pallas kernels for 0% -> 0%
where the time goes in v1:
time: 82.7 us; the launch traced here: 81.6 us
  Pallas kernels  72.4 us (88%)
  local copies, waits for them, and re-layouts  8.46 us (10%)
    pallas_call x1, Pallas kernels, body(): pl.pallas_call(exchange_kernel, out_shape=(pltpu.VMEM(by_z, bf16), pltpu....  70.2 us
    unnamed x22, local copies, waits for them, and re-layouts  8.46 us
    pallas_call x1, Pallas kernels, body(): pl.pallas_call(update_kernel, out_shape=one + one, in_specs=[vmem] * 8, o...  2.24 us

profile of v1, /device:TPU:1, one launch (start us, length us, event | category | flops | bytes accessed | tf_op | source)
XLA Modules:
  0.0 81.6 jit_solution(7648608511263528426)
XLA Ops:
  0.6 0.0 copy-start
  0.7 1.1 %copy-done = bf16[192,2048]{1,0:T(8,128)(2,1)S(1)} copy-done((bf16[192,2048]{1,0:T(8,128)(2,1)S(1)}, bf16[192,2048]{1,0:T(8,128)(2,1)}, u32[]{:S(2)}) %copy-start) | copy-done | bytes 786456
  1.8 0.0 copy-start.1
  1.8 0.9 %copy-done.1 = bf16[192,256]{1,0:T(8,128)(2,1)S(1)} copy-done((bf16[192,256]{1,0:T(8,128)(2,1)S(1)}, bf16[192,256]{1,0:T(8,128)(2,1)}, u32[]{:S(2)}) %copy-start.1) | copy-done | bytes 98328
  2.7 0.0 copy-start.2
  2.7 0.9 %copy-done.2 = bf16[192,256]{1,0:T(8,128)(2,1)S(1)} copy-done((bf16[192,256]{1,0:T(8,128)(2,1)S(1)}, bf16[192,256]{1,0:T(8,128)(2,1)}, u32[]{:S(2)}) %copy-start.2) | copy-done | bytes 98328
  3.6 0.0 copy-start.3
  3.6 0.7 copy-done.3
  4.3 0.0 copy-start.4
  4.3 0.7 copy-done.4
  5.0 0.0 copy-start.5
  5.0 0.7 copy-done.5
  5.7 0.0 copy-start.6
  5.7 0.7 copy-done.6
  6.4 0.0 copy-start.7
  6.4 0.7 copy-done.7
  7.1 0.0 copy-start.8
  7.1 0.7 copy-done.8
  7.8 0.0 copy-start.9
  7.8 0.7 copy-done.9
  8.4 0.0 copy-start.10
  8.4 0.7 copy-done.10
  9.1 70.2 %shard_map.186 = (bf16[8,4,2,2,16,256]{5,4,3,2,1,0:T(8,128)(2,1)S(1)}, bf16[4,2,8,2,16,256]{5,4,3,2,1,0:T(8,128)(2,1)S(1)}, f32[8,4,2,2,16,256]{5,4,3,2,1,0:T(8,...) custom-call(bf16[192,2048]{1,0:T(8,128)(2,1)S(1)} %copy-done, ...), custom_call_target="tpu_custom_call" | custom-call | tf_op jit(solution)/shard_map/pallas_call | solution.py:386
  79.3 2.2 %shard_map.187 = (f32[16,256]{1,0:T(8,128)}, f32[16,256]{1,0:T(8,128)}, bf16[2048,256]{1,0:T(8,128)(2,1)}, f32[2,256]{1,0:T(2,128)}, f32[2,256]{1,0:T(2,128)}, /...) custom-call(bf16[8,4,2,2,16,256]{5,4,3,2,1,0:T(8,128)(2,1)S(1)} %get, ...), custom_call_target="tpu_custom_call" | custom-call | tf_op jit(solution)/shard_map/pallas_call | solution.py:413
Async XLA Ops:
  0.6 1.1 %copy-start = (bf16[192,2048]{1,0:T(8,128)(2,1)S(1)}, bf16[192,2048]{1,0:T(8,128)(2,1)}, u32[]{:S(2)}) copy-start(bf16[192,2048]{1,0:T(8,128)(2,1)} %x_hbm.1) | copy-start | bytes 2359300
  1.8 0.9 %copy-start.1 = (bf16[192,256]{1,0:T(8,128)(2,1)S(1)}, bf16[192,256]{1,0:T(8,128)(2,1)}, u32[]{:S(2)}) copy-start(bf16[192,256]{1,0:T(8,128)(2,1)} %cq_hbm.1) | copy-start | bytes 294916
  2.7 0.9 %copy-start.2 = (bf16[192,256]{1,0:T(8,128)(2,1)S(1)}, bf16[192,256]{1,0:T(8,128)(2,1)}, u32[]{:S(2)}) copy-start(bf16[192,256]{1,0:T(8,128)(2,1)} %ck_hbm.1) | copy-start | bytes 294916
  3.6 0.7 copy-start.3
  4.3 0.7 copy-start.4
  5.0 0.7 copy-start.5
  5.7 0.7 copy-start.6
  6.4 0.7 copy-start.7
  7.1 0.7 copy-start.8
  7.8 0.7 copy-start.9
  8.4 0.7 copy-start.10

commit v2 on v1

v2 whole, which is shorter than its diff:
```python
import jax
import jax.numpy as jnp
from jax import lax
from jax.experimental import pallas as pl
from jax.experimental.pallas import tpu as pltpu
from jax.sharding import Mesh
from jax.sharding import PartitionSpec as P

MESH = pl.DeviceIdType.MESH
FS = ("z", "y", "c")
N = 8
SUBS = 4
FAR_FIRST = (4, 3, 5, 2, 6, 1, 7)

beta_one = 0.9
beta_two = 0.99
denom_floor = 0.001
scale_floor = 0.5
learn_rate = 0.02

f32 = jnp.float32
bf16 = jnp.bfloat16


def two_pieces(v):
    high = v.astype(bf16)
    low = (v - high.astype(f32)).astype(bf16)
    return high, low


def ring(v, d):
    return lax.rem(v + (d + 2 * N), N)


class Part:
    def __init__(self, first, second, pos):
        self.first, self.second = first, second
        self.f, self.s, self.c = pos[first], pos[second], pos["c"]
        self.by_z = second == "z"

    def block(self, buf, f, s, c):
        return buf.at[s, f // 2, f % 2, c] if self.by_z else buf.at[f // 2, f % 2, s, c]

    def sub(self, buf, j, s, c):
        return buf.at[s, j, :, c] if self.by_z else buf.at[j, :, s, c]

    def half(self, buf, h, s, c):
        return buf.at[s, pl.ds(2 * h, 2), :, c] if self.by_z else buf.at[pl.ds(2 * h, 2), :, s, c]

    def strip(self, buf, s, c):
        return buf.at[s, :, :, c] if self.by_z else buf.at[:, :, s, c]

    def one_core(self, buf):
        return buf.at[:, :, :, 0]

    def peer(self, axis, d):
        return {axis: ring(self.f if axis == self.first else self.s, d)}


def rows_of(buf, k, b):
    return (buf[b] if k == 0 else buf[b // 2, b % 2]).reshape(256, 256)


def own_rows(buf, k, z, y, c):
    return buf[z, y // 2, y % 2, c] if k == 0 else buf[z // 2, z % 2, y, c]


def exchange_kernel(
    x_hbm, cq_hbm, ck_hbm, fq_hbm, fk_hbm, q1_hbm, q2_hbm, k1_hbm, k2_hbm, wq_hbm, wk_hbm,
    FQ, FK, WQ, WK, DQ, DK, total_ref, mom_ref,
    xv, cots, fown, MQ, MK, MF, PB, PR, SB, R1, R2, SX, TT, T, M8,
    loc, out, d1, r2, dd, w1, wr, wl, wd, ms, ps, b1, b2, c1, cd, xs, ts,
):
    pos = {a: lax.axis_index(a) for a in FS}
    x = lax.axis_index("tp")
    z, y, c = pos["z"], pos["y"], pos["c"]
    parts = (Part("y", "z", pos), Part("z", "y", pos))
    both = tuple(enumerate(parts))
    F, W, Dn, Mo = (FQ, FK), (WQ, WK), (DQ, DK), (MQ, MK)
    other = {"c": 1 - c}

    def send(src, dst, group, recv, to):
        pltpu.make_async_remote_copy(
            src_ref=src, dst_ref=dst, send_sem=out.at[group], recv_sem=recv, device_id=to, device_id_type=MESH
        ).start()

    def arrived(view, recv):
        pltpu.make_async_copy(view, view, recv).wait()

    def load(src, dst, sem):
        pltpu.make_async_copy(src, dst, loc.at[sem]).start()

    load(fq_hbm, fown.at[0], 0)
    load(fk_hbm, fown.at[1], 0)
    load(q1_hbm, MQ.at[z, 0], 1)
    load(q2_hbm, MQ.at[z, 1], 1)
    load(k1_hbm, MK.at[y, 0], 2)
    load(k2_hbm, MK.at[y, 1], 2)
    load(wq_hbm, parts[0].block(WQ, y, z, c), 3)
    load(wk_hbm, parts[1].block(WK, z, y, c), 3)
    load(cq_hbm, cots.at[0], 4)
    load(ck_hbm, cots.at[1], 4)
    load(x_hbm, xv, 5)

    barrier = pltpu.get_barrier_semaphore()
    greeted = [{"y": ring(y, d)} for d in range(1, N)] + [{"z": ring(z, d)} for d in range(1, N)] + [other]
    kin = []
    for d in range(1, 4):
        kin += [{"tp": lax.rem(x + d, 4)}, {"tp": lax.rem(x + d, 4), "c": 1 - c}]
    for to in greeted + kin:
        pl.semaphore_signal(barrier, inc=1, device_id=to, device_id_type=MESH)

    rank = lax.broadcasted_iota(jnp.int32, (256, 256), 0)
    slot = lax.broadcasted_iota(jnp.int32, (256, 256), 1)
    sf, sc, ss, si = slot >> 5, (slot >> 4) & 1, (slot >> 1) & 7, slot & 1
    places = (((ss * 8 + sf) * 2 + sc) * 2 + si, ((sf * 8 + ss) * 2 + sc) * 2 + si)
    arrived(fown, loc.at[0])
    for k, p in both:
        order = jnp.where(rank == places[k], 1.0, 0.0).astype(bf16)
        mine = jnp.dot(fown[k], order, preferred_element_type=f32).astype(bf16)
        p.block(F[k], p.f, p.s, c)[...] = mine
    arrived(MQ.at[0], loc.at[1])
    arrived(MK.at[0], loc.at[2])
    arrived(WQ.at[0, 0, :, 0], loc.at[3])
    pl.semaphore_wait(barrier, len(greeted) + len(kin))

    def direct(k, buf, group, recv_of):
        p = parts[k]
        mine = p.block(buf, p.f, p.s, c)
        for d in FAR_FIRST:
            send(mine, mine, group, recv_of(k, p, d), p.peer(p.first, d))

    def pair_sem(k, p, d):
        return d1.at[k, lax.rem(p.f // 2 - ring(p.f, d) // 2 + SUBS, SUBS)]

    for k in (0, 1):
        direct(k, F[k], 0, pair_sem)

    def piece(p, n):
        return lax.rem(p.f // 2 + n, SUBS)

    for n in range(SUBS):
        for k, p in both:
            j = piece(p, n)
            mine = p.sub(F[k], j, p.s, c)
            arrived(p.block(F[k], 0, 0, 0) if n == 0 else mine, d1.at[k, n])
            for d in (2, -2, 1, -1):
                send(mine, mine, 1, r2.at[k, d + 3, n // 2], p.peer(p.second, d))
    for k, p in both:
        mine = p.strip(F[k], p.s, c)
        send(mine, mine, 2, dd.at[k], other)
    for h in (0, 1):
        for k, p in both:
            for way in (1, -1):
                src = ring(p.s, -2 * way)
                arrived(p.half(F[k], 0, src, c), r2.at[k, 2 * way + 3, h])
                for n in (2 * h, 2 * h + 1):
                    got = p.sub(F[k], piece(p, n), src, c)
                    if (h == 0) == (way == 1):
                        send(got, got, 1, r2.at[k, 7, h], p.peer(p.second, 2 * way))
                    send(got, got, 1, r2.at[k, 3 * way + 3, h], p.peer(p.second, way))
    for k, p in both:
        for d in (1, -1):
            for h in (0, 1):
                arrived(p.half(F[k], 0, p.s, c), r2.at[k, d + 3, h])
        for d in (1, -1, 2, -2):
            got = p.strip(F[k], ring(p.s, d), c)
            send(got, got, 2, dd.at[k], other)

    for k, p in both:
        for d in FAR_FIRST:
            mine = Mo[k].at[p.s]
            send(mine, mine, 3 + k, ms.at[k], p.peer(p.second, d))
    for k in (0, 1):
        direct(k, W[k], 5, lambda k, p, d: w1.at[k])

    for k, p in both:
        for d in (3, -3, 4):
            for h in (0, 1):
                arrived(p.half(F[k], 0, p.s, c), r2.at[k, d + 3, h])
            got = p.strip(F[k], ring(p.s, -d), c)
            send(got, got, 2, dd.at[k], other)

    def weights_step(t):
        for k, p in both:
            right, left = p.peer(p.second, 1), p.peer(p.second, -1)
            if t == 0:
                arrived((WQ.at[pl.ds(0, 7), 0, 0, 0]), w1.at[k])
                mine = p.strip(W[k], p.s, c)
                send(mine, mine, 6, wr.at[k, 0], right)
                send(mine, mine, 6, wl.at[k, 0], left)
                send(mine, mine, 7, wd.at[k], other)
            elif t < 4:
                from_left = p.strip(W[k], ring(p.s, -t), c)
                arrived(from_left, wr.at[k, t - 1])
                from_right = p.strip(W[k], ring(p.s, t), c)
                arrived(from_right, wl.at[k, t - 1])
                if t < 3:
                    send(from_left, from_left, 6, wr.at[k, t], right)
                    send(from_right, from_right, 6, wl.at[k, t], left)
                else:
                    low, high = p.half(W[k], 0, ring(p.s, -3), c), p.half(W[k], 1, ring(p.s, 3), c)
                    send(low, low, 6, wr.at[k, 3], right)
                    send(high, high, 6, wl.at[k, 3], left)
                send(from_left, from_left, 7, wd.at[k], other)
                send(from_right, from_right, 7, wd.at[k], other)
            else:
                arrived(p.half(W[k], 0, ring(p.s, 4), c), wr.at[k, 3])
                arrived(p.half(W[k], 1, ring(p.s, 4), c), wl.at[k, 3])
                last = p.strip(W[k], ring(p.s, 4), c)
                send(last, last, 7, wd.at[k], other)

    arrived(cots, loc.at[4])
    arrived(xv, loc.at[5])
    for k, p in both:
        arrived(p.one_core(F[k]), dd.at[k])
        mixed = jnp.zeros((192, 256), f32)
        for b in range(N):
            mixed += jnp.dot(xv[:, b * 256 : (b + 1) * 256], rows_of(F[k], k, b), preferred_element_type=f32)
        high, low = two_pieces(mixed)
        product = jnp.dot(high.T, cots[k], preferred_element_type=f32)
        product += jnp.dot(low.T, cots[k], preferred_element_type=f32)
        PB[k] = product.reshape(N, 2, 16, 256)
        send(PB.at[k, :, 1 - c], PR.at[k], 8, ps.at[k], other)
    weights_step(0)

    for k, p in both:
        arrived(PR.at[k], ps.at[k])
        SB[k] = PB[k, :, c] + PR[k]
        for d in FAR_FIRST:
            to = ring(p.f, d)
            send(SB.at[k, to], R1.at[k, p.f], 9, b1.at[k], {p.first: to})
    weights_step(1)
    for k, p in both:
        arrived(R1.at[k, pl.ds(0, 7)], b1.at[k])
        acc = SB[k, p.f]
        for d in FAR_FIRST:
            acc += R1[k, ring(p.f, -d)]
        R2[k, p.s] = acc
        for d in FAR_FIRST:
            mine = R2.at[k, p.s]
            send(mine, mine, 10, b2.at[k], p.peer(p.second, d))
    for k, p in both:
        arrived(Mo[k].at[pl.ds(0, 7)], ms.at[k])
        for b in range(N):
            for m in (0, 1):
                MF[k, m, 2 * b : 2 * b + 2, :] = Mo[k][b, m]
    weights_step(2)

    sums = []
    for k, p in both:
        arrived(R2.at[k, pl.ds(0, 7)], b2.at[k])
        small = R2[k, 0]
        for b in range(1, N):
            small += R2[k, b]
        first_new = beta_one * MF[k, 0] + (1.0 - beta_one) * small
        second_new = beta_two * MF[k, 1] + (1.0 - beta_two) * small * small
        direction = first_new / (jnp.sqrt(second_new) + denom_floor)
        Dn[k][p.f, c] = direction
        for d in FAR_FIRST:
            mine = Dn[k].at[p.f, c]
            send(mine, mine, 11, c1.at[k], p.peer(p.first, d))
        sums.append(jnp.sum(direction * direction, axis=(0, 1), keepdims=True))
        T[k, 0] = first_new
        T[k, 1] = second_new

    row = lax.broadcasted_iota(jnp.int32, (2, 128), 0)
    SX[2 * x + c] = jnp.where(row == 0, sums[0], sums[1])
    for to in [other] + kin:
        mine = SX.at[2 * x + c]
        send(mine, mine, 13, xs.at[0], to)
    for k, p in both:
        for m in (0, 1):
            for b in range(N):
                M8[k, m, b] = T[k, m, 2 * b : 2 * b + 2, :]
            mom_ref[k, m] = M8[k, m, p.s]
    arrived(SX.at[pl.ds(0, 7)], xs.at[0])
    across = SX[0]
    for b in range(1, N):
        across += SX[b]
    for k, p in both:
        TT[k, p.f] = across
        for d in FAR_FIRST:
            mine = TT.at[k, p.f]
            send(mine, mine, 14, ts.at[k], p.peer(p.first, d))
    weights_step(3)
    for k, p in both:
        arrived(DQ.at[pl.ds(0, 7), 0], c1.at[k])
        mine = Dn[k].at[:, c]
        send(mine, mine, 12, cd.at[k], other)
    weights_step(4)
    totals = []
    for k in (0, 1):
        arrived(TT.at[k, pl.ds(0, 7)], ts.at[k])
        total = TT[k, 0]
        for b in range(1, N):
            total += TT[k, b]
        totals.append(total[k : k + 1, 0:1])
    lane = lax.broadcasted_iota(jnp.int32, (8, 256), 0)
    total_ref[...] = jnp.where(lane == 0, totals[0], totals[1])
    for k, p in both:
        arrived(DQ.at[:, 0], cd.at[k])
        arrived(p.one_core(W[k]), wd.at[k])

    arrived(FQ.at[pl.ds(0, 7), 0, :, 0], out.at[0])
    arrived(FQ.at[pl.ds(0, 7)], out.at[1])
    arrived(FQ, out.at[2])
    arrived(MQ.at[pl.ds(0, 7)], out.at[3])
    arrived(MQ.at[pl.ds(0, 7)], out.at[4])
    arrived(WQ.at[pl.ds(0, 7), 0, :, 0], out.at[5])
    arrived(WQ.at[pl.ds(0, 7)], out.at[6])
    arrived(WQ, out.at[7])
    arrived(PB.at[:, :, 0], out.at[8])
    arrived(R1.at[:, pl.ds(0, 7)], out.at[9])
    arrived(R2.at[:, pl.ds(0, 7)], out.at[10])
    arrived(DQ.at[pl.ds(0, 7)], out.at[11])
    arrived(DQ, out.at[12])
    arrived(SX.at[pl.ds(0, 7)], out.at[13])
    arrived(TT.at[:, pl.ds(0, 7)], out.at[14])


def update_kernel(
    FQ, FK, WQ, WK, DQ, DK, total_ref, mom_ref,
    uq_out, nq_out, cq_out, f1q_out, f2q_out, uk_out, nk_out, ck_out, f1k_out, f2k_out,
    copies, own, mom, sems, small_sems,
):
    z, y, c = (lax.axis_index(a) for a in FS)
    F, W, Dn = (FQ, FK), (WQ, WK), (DQ, DK)
    outs = ((uq_out, nq_out, cq_out, f1q_out, f2q_out), (uk_out, nk_out, ck_out, f1k_out, f2k_out))
    flight = []
    mom[...] = mom_ref[...]
    for k in (0, 1):
        for m in (0, 1):
            copy = pltpu.make_async_copy(mom.at[k, m], outs[k][3 + m], small_sems.at[k, m])
            copy.start()
            flight.append(copy)
    for k in (0, 1):
        total = total_ref[k : k + 1, :]
        scale = 1.0 / jnp.maximum(jnp.sqrt(total * (1.0 / 262144.0)), scale_floor)
        high, low = two_pieces(Dn[k][...].reshape(256, 256))

        def update_of(rows):
            whole = jnp.dot(rows, high, preferred_element_type=f32) + jnp.dot(rows, low, preferred_element_type=f32)
            return -scale * whole

        for b in range(N):
            update = update_of(rows_of(F[k], k, b))
            new = rows_of(W[k], k, b) + learn_rate * update
            copies[k, b] = new.astype(bf16)
            copy = pltpu.make_async_copy(copies.at[k, b], outs[k][2].at[pl.ds(b * 256, 256), :], sems.at[k, b])
            copy.start()
            flight.append(copy)
        update = update_of(own_rows(F[k], k, z, y, c))
        own[k, 0] = update
        own[k, 1] = own_rows(W[k], k, z, y, c) + learn_rate * update
        for m in (0, 1):
            copy = pltpu.make_async_copy(own.at[k, m], outs[k][m], small_sems.at[k, 2 + m])
            copy.start()
            flight.append(copy)
    for copy in flight:
        copy.wait()


def body(*args):
    hbm = pl.BlockSpec(memory_space=pltpu.HBM)
    vmem = pl.BlockSpec(memory_space=pltpu.VMEM)
    shape = jax.ShapeDtypeStruct
    by_z, by_y = (8, 4, 2, 2, 16, 256), (4, 2, 8, 2, 16, 256)
    dma = pltpu.SemaphoreType.DMA
    room = pltpu.VMEM
    mid = pl.pallas_call(
        exchange_kernel,
        out_shape=(
            room(by_z, bf16), room(by_y, bf16), room(by_z, f32), room(by_y, f32),
            room((8, 2, 16, 256), f32), room((8, 2, 16, 256), f32), room((8, 256), f32), room((2, 2, 2, 256), f32),
        ),
        in_specs=[hbm] * 11,
        out_specs=(vmem,) * 8,
        scratch_shapes=[
            room((192, 2048), bf16), room((2, 192, 256), bf16), room((2, 16, 256), bf16),
            room((8, 2, 2, 256), f32), room((8, 2, 2, 256), f32), room((2, 2, 16, 256), f32),
            room((2, 8, 2, 16, 256), f32), room((2, 8, 16, 256), f32), room((2, 8, 16, 256), f32),
            room((2, 8, 16, 256), f32), room((2, 8, 16, 256), f32), room((8, 2, 128), f32), room((2, 8, 2, 128), f32),
            room((2, 2, 16, 256), f32), room((2, 2, 8, 2, 256), f32),
            dma((6,)), dma((15,)), dma((2, 4)), dma((2, 8, 2)), dma((2,)),
            dma((2,)), dma((2, 4)), dma((2, 4)), dma((2,)), dma((2,)), dma((2,)),
            dma((2,)), dma((2,)), dma((2,)), dma((2,)), dma((1,)), dma((2,)),
        ],
        compiler_params=pltpu.CompilerParams(collective_id=0, has_side_effects=True, vmem_limit_bytes=40 * 1024 * 1024),
    )(*(pltpu.with_memory_space_constraint(a, pltpu.HBM) for a in args))
    one = (
        shape((16, 256), f32), shape((16, 256), f32), shape((2048, 256), bf16), shape((2, 256), f32), shape((2, 256), f32),
    )
    return pl.pallas_call(
        update_kernel,
        out_shape=one + one,
        in_specs=[vmem] * 8,
        out_specs=(hbm,) * 10,
        scratch_shapes=[
            room((2, 8, 256, 256), bf16), room((2, 2, 16, 256), f32), room((2, 2, 2, 256), f32), dma((2, 8)), dma((2, 4)),
        ],
        compiler_params=pltpu.CompilerParams(vmem_limit_bytes=40 * 1024 * 1024),
    )(*mid)


def solution(mesh):
    split = Mesh(mesh.devices.reshape(8, 8, 2, mesh.shape["tp"]), ("z", "y", "c", "tp"))
    rows, tiles = P(FS, None), P(FS, "tp")
    one = (tiles, tiles, P(None, "tp"), tiles, tiles)
    return jax.shard_map(
        body,
        mesh=split,
        in_specs=(rows, tiles, tiles, rows, rows, tiles, tiles, tiles, tiles, tiles, tiles),
        out_specs=one + one,
        check_vma=False,
    )
```

time: 82.7 us -> 62.3 us (0.75); the launches traced: 81.6 us -> 62.1 us
  Pallas kernels: 72.4 us -> 61.5 us
  local copies, waits for them, and re-layouts: 8.46 us -> 0 us
    pallas_call x1, Pallas kernels: 70.2 us -> 59.2 us  [body(): pl.pallas_call(exchange_kernel, out_shape=(room(by_z, bf16), room(by_y, b...]
    unnamed x22 -> x0, local copies, waits for them, and re-layouts: 8.46 us -> none
where the time goes in v2:
time: 62.3 us; the launch traced here: 62.1 us
  Pallas kernels  61.5 us (99%)
  between operations  0.65 us (1%)
    pallas_call x1, Pallas kernels, body(): pl.pallas_call(exchange_kernel, out_shape=(room(by_z, bf16), room(by_y, b...  59.2 us
    pallas_call x1, Pallas kernels, body(): pl.pallas_call(update_kernel, out_shape=one + one, in_specs=[vmem] * 8, o...  2.24 us

profile of v2, /device:TPU:1, one launch (start us, length us, event | category | flops | bytes accessed | tf_op | source)
XLA Modules:
  0.0 62.1 jit_solution(1621327109435022754)
XLA Ops:
  0.6 59.2 %shard_map.186 = (bf16[8,4,2,2,16,256]{5,4,3,2,1,0:T(8,128)(2,1)S(1)}, bf16[4,2,8,2,16,256]{5,4,3,2,1,0:T(8,128)(2,1)S(1)}, f32[8,4,2,2,16,256]{5,4,3,2,1,0:T(8,...) custom-call(bf16[192,2048]{1,0:T(8,128)(2,1)} %x_hbm.1, ...), custom_call_target="tpu_custom_call" | custom-call | tf_op jit(solution)/shard_map/pallas_call | solution.py:371
  59.9 2.2 %shard_map.187 = (f32[16,256]{1,0:T(8,128)}, f32[16,256]{1,0:T(8,128)}, bf16[2048,256]{1,0:T(8,128)(2,1)}, f32[2,256]{1,0:T(2,128)}, f32[2,256]{1,0:T(2,128)}, /...) custom-call(bf16[8,4,2,2,16,256]{5,4,3,2,1,0:T(8,128)(2,1)S(1)} %get, ...), custom_call_target="tpu_custom_call" | custom-call | tf_op jit(solution)/shard_map/pallas_call | solution.py:394

commit v3 on v2

--- a/solution.py
+++ b/solution.py
@@ -135,6 +135,8 @@
 
     for k in (0, 1):
         direct(k, F[k], 0, pair_sem)
+    for k in (0, 1):
+        direct(k, W[k], 5, lambda k, p, d: w1.at[k])
 
     def piece(p, n):
         return lax.rem(p.f // 2 + n, SUBS)
@@ -171,16 +173,6 @@
         for d in FAR_FIRST:
             mine = Mo[k].at[p.s]
             send(mine, mine, 3 + k, ms.at[k], p.peer(p.second, d))
-    for k in (0, 1):
-        direct(k, W[k], 5, lambda k, p, d: w1.at[k])
-
-    for k, p in both:
-        for d in (3, -3, 4):
-            for h in (0, 1):
-                arrived(p.half(F[k], 0, p.s, c), r2.at[k, d + 3, h])
-            got = p.strip(F[k], ring(p.s, -d), c)
-            send(got, got, 2, dd.at[k], other)
-
     def weights_step(t):
         for k, p in both:
             right, left = p.peer(p.second, 1), p.peer(p.second, -1)
@@ -210,6 +202,15 @@
                 last = p.strip(W[k], ring(p.s, 4), c)
                 send(last, last, 7, wd.at[k], other)
 
+    weights_step(0)
+    for k, p in both:
+        for d in (3, -3, 4):
+            for h in (0, 1):
+                arrived(p.half(F[k], 0, p.s, c), r2.at[k, d + 3, h])
+                for n in (2 * h, 2 * h + 1):
+                    got = p.sub(F[k], piece(p, n), ring(p.s, -d), c)
+                    send(got, got, 2, dd.at[k], other)
+
     arrived(cots, loc.at[4])
     arrived(xv, loc.at[5])
     for k, p in both:
@@ -222,7 +223,7 @@
         product += jnp.dot(low.T, cots[k], preferred_element_type=f32)
         PB[k] = product.reshape(N, 2, 16, 256)
         send(PB.at[k, :, 1 - c], PR.at[k], 8, ps.at[k], other)
-    weights_step(0)
+    weights_step(1)
 
     for k, p in both:
         arrived(PR.at[k], ps.at[k])
@@ -230,7 +231,7 @@
         for d in FAR_FIRST:
             to = ring(p.f, d)
             send(SB.at[k, to], R1.at[k, p.f], 9, b1.at[k], {p.first: to})
-    weights_step(1)
+    weights_step(2)
     for k, p in both:
         arrived(R1.at[k, pl.ds(0, 7)], b1.at[k])
         acc = SB[k, p.f]
@@ -245,7 +246,7 @@
         for b in range(N):
             for m in (0, 1):
                 MF[k, m, 2 * b : 2 * b + 2, :] = Mo[k][b, m]
-    weights_step(2)
+    weights_step(3)
 
     sums = []
     for k, p in both:
@@ -283,12 +284,11 @@
         for d in FAR_FIRST:
             mine = TT.at[k, p.f]
             send(mine, mine, 14, ts.at[k], p.peer(p.first, d))
-    weights_step(3)
+    weights_step(4)
     for k, p in both:
         arrived(DQ.at[pl.ds(0, 7), 0], c1.at[k])
         mine = Dn[k].at[:, c]
         send(mine, mine, 12, cd.at[k], other)
-    weights_step(4)
     totals = []
     for k in (0, 1):
         arrived(TT.at[k, pl.ds(0, 7)], ts.at[k])

time: 62.3 us -> 60 us (0.963)
  Pallas kernels: 61.5 us -> 59.2 us
    pallas_call x1, Pallas kernels: 59.2 us -> 56.9 us  [body(): pl.pallas_call(exchange_kernel, out_shape=(room(by_z, bf16), room(by_y, b...]
where the time goes in v3:
time: 60 us; the launch traced here: 59.8 us
  Pallas kernels  59.2 us (99%)
  between operations  0.65 us (1%)
    pallas_call x1, Pallas kernels, body(): pl.pallas_call(exchange_kernel, out_shape=(room(by_z, bf16), room(by_y, b...  56.9 us
    pallas_call x1, Pallas kernels, body(): pl.pallas_call(update_kernel, out_shape=one + one, in_specs=[vmem] * 8, o...  2.24 us

profile of v3, /device:TPU:1, one launch (start us, length us, event | category | flops | bytes accessed | tf_op | source)
XLA Modules:
  0.0 59.8 jit_solution(18382200253419884045)
XLA Ops:
  0.6 56.9 %shard_map.186 = (bf16[8,4,2,2,16,256]{5,4,3,2,1,0:T(8,128)(2,1)S(1)}, bf16[4,2,8,2,16,256]{5,4,3,2,1,0:T(8,128)(2,1)S(1)}, f32[8,4,2,2,16,256]{5,4,3,2,1,0:T(8,...) custom-call(bf16[192,2048]{1,0:T(8,128)(2,1)} %x_hbm.1, ...), custom_call_target="tpu_custom_call" | custom-call | tf_op jit(solution)/shard_map/pallas_call | solution.py:371
  57.6 2.2 %shard_map.187 = (f32[16,256]{1,0:T(8,128)}, f32[16,256]{1,0:T(8,128)}, bf16[2048,256]{1,0:T(8,128)(2,1)}, f32[2,256]{1,0:T(2,128)}, f32[2,256]{1,0:T(2,128)}, /...) custom-call(bf16[8,4,2,2,16,256]{5,4,3,2,1,0:T(8,128)(2,1)S(1)} %get, ...), custom_call_target="tpu_custom_call" | custom-call | tf_op jit(solution)/shard_map/pallas_call | solution.py:394

commit v4 on v3

v4 whole, which is shorter than its diff:
```python
import jax
import jax.numpy as jnp
from jax import lax
from jax.experimental import pallas as pl
from jax.experimental.pallas import tpu as pltpu
from jax.sharding import Mesh
from jax.sharding import PartitionSpec as P

MESH = pl.DeviceIdType.MESH
FS = ("z", "y", "c")
N = 8
FAR_FIRST = (4, 3, 5, 2, 6, 1, 7)
NEAR_FIRST = (1, 7, 2, 6, 3, 5, 4)

beta_one = 0.9
beta_two = 0.99
denom_floor = 0.001
scale_floor = 0.5
learn_rate = 0.02

f32 = jnp.float32
bf16 = jnp.bfloat16


def two_pieces(v):
    high = v.astype(bf16)
    low = (v - high.astype(f32)).astype(bf16)
    return high, low


def ring(v, d):
    return lax.rem(v + (d + 2 * N), N)


class Part:
    def __init__(self, first, second, pos):
        self.first, self.second = first, second
        self.f, self.s, self.c = pos[first], pos[second], pos["c"]
        self.by_z = second == "z"

    def block(self, buf, f, s, c):
        return buf.at[s, f // 2, f % 2, c] if self.by_z else buf.at[f // 2, f % 2, s, c]

    def half(self, buf, h, s, c):
        return buf.at[s, pl.ds(2 * h, 2), :, c] if self.by_z else buf.at[pl.ds(2 * h, 2), :, s, c]

    def strip(self, buf, s, c):
        return buf.at[s, :, :, c] if self.by_z else buf.at[:, :, s, c]

    def one_core(self, buf):
        return buf.at[:, :, :, 0]

    def peer(self, axis, d):
        return {axis: ring(self.f if axis == self.first else self.s, d)}


def assemble(FULL, plane, b):
    pair = jnp.stack([FULL[plane, 0, b], FULL[plane, 1, :, b]], axis=1)
    return pair.reshape(256, 128)


def rows_of(buf, k, b):
    return (buf[b] if k == 0 else buf[b // 2, b % 2]).reshape(256, 256)


def own_rows(buf, k, z, y, c):
    return buf[z, y // 2, y % 2, c] if k == 0 else buf[z // 2, z % 2, y, c]


def exchange_kernel(
    x_hbm, cq_hbm, ck_hbm, fq_hbm, fk_hbm, q1_hbm, q2_hbm, k1_hbm, k2_hbm, wq_hbm, wk_hbm,
    FULL, WQ, WK, DD, total_ref, mom_ref,
    xv, cots, CA, fown, MOM, MF, PB, PR, SB, R1, S1, R2, TS, T, M8,
    loc, out, inn, r2, w1, wr, wl, wd,
):
    pos = {a: lax.axis_index(a) for a in FS}
    x = lax.axis_index("tp")
    z, y, c = pos["z"], pos["y"], pos["c"]
    both = tuple(enumerate((Part("y", "z", pos), Part("z", "y", pos))))
    W = (WQ, WK)
    other = {"c": 1 - c}
    first_is_y = c == 0
    f, s = jnp.where(first_is_y, y, z), jnp.where(first_is_y, z, y)
    proj, side = x // 2, x % 2
    D1, DDUP, MS, CS, PS, B1, B2, C1, CD, TSUM, FX, FD = range(12)

    def on_first(d):
        return {"y": jnp.where(first_is_y, ring(y, d), y), "z": jnp.where(first_is_y, z, ring(z, d))}

    def on_second(d):
        return {"y": jnp.where(first_is_y, y, ring(y, d)), "z": jnp.where(first_is_y, ring(z, d), z)}

    def plane(d):
        return lax.rem(x + d, 4)

    def send(src, dst, group, recv, to):
        pltpu.make_async_remote_copy(
            src_ref=src, dst_ref=dst, send_sem=out.at[group], recv_sem=recv, device_id=to, device_id_type=MESH
        ).start()

    def same(ref, group, recv, to):
        send(ref, ref, group, recv, to)

    def arrived(view, recv):
        pltpu.make_async_copy(view, view, recv).wait()

    def load(src, dst, sem):
        pltpu.make_async_copy(src, dst, loc.at[sem]).start()

    load(fq_hbm, fown.at[0], 0)
    load(fk_hbm, fown.at[1], 0)
    load(cq_hbm, cots.at[0], 4)
    load(ck_hbm, cots.at[1], 4)
    load(wq_hbm, both[0][1].block(WQ, y, z, c), 3)
    load(wk_hbm, both[1][1].block(WK, z, y, c), 3)
    load(q1_hbm, MOM.at[s, 0, 0], 1)
    load(q2_hbm, MOM.at[s, 0, 1], 1)
    load(k1_hbm, MOM.at[s, 1, 0], 1)
    load(k2_hbm, MOM.at[s, 1, 1], 1)

    @pl.when(proj == 0)
    def _():
        load(cq_hbm, CA.at[x], 2)

    @pl.when(proj == 1)
    def _():
        load(ck_hbm, CA.at[x], 2)

    load(x_hbm, xv, 5)

    barrier = pltpu.get_barrier_semaphore()
    greeted = [{"y": ring(y, d)} for d in range(1, N)] + [{"z": ring(z, d)} for d in range(1, N)] + [other]
    for d in range(1, 4):
        greeted += [{"tp": plane(d)}, {"tp": plane(d), "c": 1 - c}]
    for to in greeted:
        pl.semaphore_signal(barrier, inc=1, device_id=to, device_id_type=MESH)

    rank = lax.broadcasted_iota(jnp.int32, (256, 128), 0)
    lane = lax.broadcasted_iota(jnp.int32, (256, 128), 1)
    lc, lf, ls, li = lane >> 6, (lane >> 3) & 7, ((lane >> 1) & 3) + 4 * side, lane & 1
    lz, ly = jnp.where(lc == 0, ls, lf), jnp.where(lc == 0, lf, ls)
    order = jnp.where(rank == ((lz * 8 + ly) * 2 + lc) * 2 + li, 1.0, 0.0).astype(bf16)
    arrived(fown, loc.at[0])
    FULL[x, c, s, f] = jnp.dot(fown[proj], order, preferred_element_type=f32).astype(bf16)
    arrived(cots, loc.at[4])
    arrived(WQ.at[0, 0, :, 0], loc.at[3])
    arrived(MOM.at[0], loc.at[1])
    pl.semaphore_wait(barrier, len(greeted))

    for d in FAR_FIRST:
        same(FULL.at[x, c, s, f], 0, inn.at[D1], on_first(d))
    for d in (2, 1, 3):
        send(cots.at[plane(d) // 2], CA.at[x], 4, inn.at[CS], {"tp": plane(d)})
    for k, p in both:
        mine = p.block(W[k], p.f, p.s, c)
        for d in FAR_FIRST:
            same(mine, 5, w1.at[k], p.peer(p.first, d))
    for d in FAR_FIRST:
        same(MOM.at[s], 3, inn.at[MS], on_second(d))

    arrived(FULL.at[0, 0, 0, pl.ds(0, 7)], inn.at[D1])
    for d in FAR_FIRST:
        same(FULL.at[x, c, s], 1, r2.at[d], on_second(d))
    same(FULL.at[x, c, s], 2, inn.at[DDUP], other)

    def weights_step(t):
        for k, p in both:
            right, left = p.peer(p.second, 1), p.peer(p.second, -1)
            if t == 0:
                arrived(WQ.at[pl.ds(0, 7), 0, 0, 0], w1.at[k])
                mine = p.strip(W[k], p.s, c)
                same(mine, 6, wr.at[k, 0], right)
                same(mine, 6, wl.at[k, 0], left)
                same(mine, 7, wd.at[k], other)
            elif t < 4:
                from_left = p.strip(W[k], ring(p.s, -t), c)
                arrived(from_left, wr.at[k, t - 1])
                from_right = p.strip(W[k], ring(p.s, t), c)
                arrived(from_right, wl.at[k, t - 1])
                if t < 3:
                    same(from_left, 6, wr.at[k, t], right)
                    same(from_right, 6, wl.at[k, t], left)
                else:
                    same(p.half(W[k], 0, ring(p.s, -3), c), 6, wr.at[k, 3], right)
                    same(p.half(W[k], 1, ring(p.s, 3), c), 6, wl.at[k, 3], left)
                same(from_left, 7, wd.at[k], other)
                same(from_right, 7, wd.at[k], other)
            else:
                arrived(p.half(W[k], 0, ring(p.s, 4), c), wr.at[k, 3])
                arrived(p.half(W[k], 1, ring(p.s, 4), c), wl.at[k, 3])
                same(p.strip(W[k], ring(p.s, 4), c), 7, wd.at[k], other)

    weights_step(0)
    for d in NEAR_FIRST:
        arrived(FULL.at[0, 0, 0], r2.at[d])
        same(FULL.at[x, c, ring(s, -d)], 2, inn.at[DDUP], other)
    for d in (2, 1, 3):
        same(FULL.at[x, c], 14, inn.at[FX], {"tp": plane(d)})

    arrived(xv, loc.at[5])
    arrived(CA.at[0], loc.at[2])
    arrived(CA.at[pl.ds(0, 3)], inn.at[CS])
    arrived(FULL.at[0, 0], inn.at[DDUP])
    mixed = jnp.zeros((192, 128), f32)
    for b in range(N):
        mixed += jnp.dot(xv[:, b * 256 : (b + 1) * 256], assemble(FULL, x, b), preferred_element_type=f32)
    high, low = two_pieces(mixed)
    pieces = jnp.concatenate([high.T, low.T], axis=0)
    for b in range(4):
        product = jnp.dot(pieces, CA[b], preferred_element_type=f32)
        PB[:, :, b] = (product[:128] + product[128:]).reshape(2, N, 8, 256)
        send(PB.at[1 - c, :, b], PR.at[:, b], 8, inn.at[PS], other)
    weights_step(1)

    arrived(PR, inn.at[PS])
    SB[...] = PB[c] + PR[...]
    for d in FAR_FIRST:
        send(SB.at[ring(f, d)], R1.at[f], 9, inn.at[B1], on_first(d))
    weights_step(2)
    arrived(R1.at[pl.ds(0, 7)], inn.at[B1])
    acc = SB[f]
    for d in FAR_FIRST:
        acc += R1[ring(f, -d)]
    S1[...] = acc

    for d in FAR_FIRST + (0,):
        for e in (2, 1, 3, 0):
            if d or e:
                send(S1.at[plane(e)], R2.at[x * N + s], 10, inn.at[B2], {**on_second(d), "tp": plane(e)})
    R2[x * N + s] = S1[x]
    weights_step(3)
    arrived(FULL.at[pl.ds(0, 3), 0], inn.at[FX])
    for d in (1, 2, 3):
        same(FULL.at[plane(d), c], 15, inn.at[FD], other)
    arrived(MOM.at[pl.ds(0, 7)], inn.at[MS])
    for k in (0, 1):
        for m in (0, 1):
            for b in range(N):
                MF[k, m, b // 4, 2 * (b % 4) : 2 * (b % 4) + 2, :] = MOM[b, k, m]

    arrived(R2.at[pl.ds(0, 31)], inn.at[B2])
    sums = []
    for k in (0, 1):
        squares = 0.0
        for h in (0, 1):
            at = (2 * k + h) * N
            small = R2[at]
            for b in range(1, N):
                small += R2[at + b]
            first_new = beta_one * MF[k, 0, h] + (1.0 - beta_one) * small
            second_new = beta_two * MF[k, 1, h] + (1.0 - beta_two) * small * small
            direction = first_new / (jnp.sqrt(second_new) + denom_floor)
            DD[c, f, k, h] = direction
            squares += direction * direction
            T[k, 0, h] = first_new
            T[k, 1, h] = second_new
        sums.append(jnp.sum(squares, axis=(0, 1), keepdims=True))
    for d in FAR_FIRST:
        same(DD.at[c, f], 11, inn.at[C1], on_first(d))

    row = lax.broadcasted_iota(jnp.int32, (2, 128), 0)
    mine = (c * N + f) * 4 + x
    TS[mine] = jnp.where(row == 0, sums[0], sums[1])
    for d in FAR_FIRST + (0,):
        for e in (2, 1, 3, 0):
            for core in (c, 1 - c):
                if d or e or core is not c:
                    same(TS.at[mine], 13, inn.at[TSUM], {**on_first(d), "tp": plane(e), "c": core})
    weights_step(4)
    for k in (0, 1):
        for m in (0, 1):
            for b in range(N):
                M8[k, m, b] = T[k, m, b // 4, 2 * (b % 4) : 2 * (b % 4) + 2, :]
            mom_ref[k, m] = M8[k, m, s]
    arrived(DD.at[0, pl.ds(0, 7)], inn.at[C1])
    same(DD.at[c], 12, inn.at[CD], other)
    arrived(TS.at[pl.ds(0, 63)], inn.at[TSUM])
    total = TS[0]
    for b in range(1, 64):
        total += TS[b]
    line = lax.broadcasted_iota(jnp.int32, (8, 256), 0)
    total_ref[...] = jnp.where(line == 0, total[0:1, 0:1], total[1:2, 0:1])
    arrived(DD.at[0], inn.at[CD])
    arrived(FULL.at[pl.ds(0, 3), 0], inn.at[FD])
    for k, p in both:
        arrived(p.one_core(W[k]), wd.at[k])

    for group, view in enumerate((
        FULL.at[0, 0, 0, pl.ds(0, 7)], FULL.at[0, 0, pl.ds(0, 7)], FULL.at[0, 0], MOM.at[pl.ds(0, 7)],
        CA.at[pl.ds(0, 3)], WQ.at[pl.ds(0, 7), 0, :, 0], WQ.at[pl.ds(0, 7)], WQ, PB.at[0], R1.at[pl.ds(0, 7)],
        R2.at[pl.ds(0, 31)], DD.at[0, pl.ds(0, 7)], DD.at[0], TS.at[pl.ds(0, 63)],
        FULL.at[pl.ds(0, 3), 0], FULL.at[pl.ds(0, 3), 0],
    )):
        arrived(view, out.at[group])


def update_kernel(
    FULL, WQ, WK, DD, total_ref, mom_ref,
    uq_out, nq_out, cq_out, f1q_out, f2q_out, uk_out, nk_out, ck_out, f1k_out, f2k_out,
    copies, own, mom, sems, small_sems,
):
    z, y, c = (lax.axis_index(a) for a in FS)
    f, s = jnp.where(c == 0, y, z), jnp.where(c == 0, z, y)
    W = (WQ, WK)
    outs = ((uq_out, nq_out, cq_out, f1q_out, f2q_out), (uk_out, nk_out, ck_out, f1k_out, f2k_out))
    flight = []
    mom[...] = mom_ref[...]
    for k in (0, 1):
        for m in (0, 1):
            copy = pltpu.make_async_copy(mom.at[k, m], outs[k][3 + m], small_sems.at[k, m])
            copy.start()
            flight.append(copy)
    for k in (0, 1):
        total = total_ref[k : k + 1, :]
        scale = 1.0 / jnp.maximum(jnp.sqrt(total * (1.0 / 262144.0)), scale_floor)
        full = jnp.concatenate([DD[:, :, k, h].reshape(128, 256) for h in (0, 1)], axis=0)
        high, low = two_pieces(full)

        def update_of(rows):
            whole = jnp.dot(rows, high, preferred_element_type=f32) + jnp.dot(rows, low, preferred_element_type=f32)
            return -scale * whole

        for b in range(N):
            rows = jnp.concatenate([assemble(FULL, 2 * k, b), assemble(FULL, 2 * k + 1, b)], axis=1)
            new = rows_of(W[k], k, b) + learn_rate * update_of(rows)
            copies[k, b] = new.astype(bf16)
            copy = pltpu.make_async_copy(copies.at[k, b], outs[k][2].at[pl.ds(b * 256, 256), :], sems.at[k, b])
            copy.start()
            flight.append(copy)
        update = update_of(jnp.concatenate([FULL[2 * k, c, s, f], FULL[2 * k + 1, c, s, f]], axis=1))
        own[k, 0] = update
        own[k, 1] = own_rows(W[k], k, z, y, c) + learn_rate * update
        for m in (0, 1):
            copy = pltpu.make_async_copy(own.at[k, m], outs[k][m], small_sems.at[k, 2 + m])
            copy.start()
            flight.append(copy)
    for copy in flight:
        copy.wait()


def body(*args):
    hbm = pl.BlockSpec(memory_space=pltpu.HBM)
    vmem = pl.BlockSpec(memory_space=pltpu.VMEM)
    shape = jax.ShapeDtypeStruct
    by_z, by_y = (8, 4, 2, 2, 16, 256), (4, 2, 8, 2, 16, 256)
    dma = pltpu.SemaphoreType.DMA
    room = pltpu.VMEM
    mid = pl.pallas_call(
        exchange_kernel,
        out_shape=(
            room((4, 2, 8, 8, 16, 128), bf16), room(by_z, f32), room(by_y, f32),
            room((2, 8, 2, 2, 8, 256), f32), room((8, 256), f32), room((2, 2, 2, 256), f32),
        ),
        in_specs=[hbm] * 11,
        out_specs=(vmem,) * 6,
        scratch_shapes=[
            room((192, 2048), bf16), room((2, 192, 256), bf16), room((4, 192, 256), bf16), room((2, 16, 256), bf16),
            room((8, 2, 2, 2, 256), f32), room((2, 2, 2, 8, 256), f32),
            room((2, 8, 4, 8, 256), f32), room((8, 4, 8, 256), f32), room((8, 4, 8, 256), f32), room((8, 4, 8, 256), f32),
            room((4, 8, 256), f32), room((32, 8, 256), f32), room((64, 2, 128), f32),
            room((2, 2, 2, 8, 256), f32), room((2, 2, 8, 2, 256), f32),
            dma((6,)), dma((16,)), dma((12,)), dma((8,)), dma((2,)), dma((2, 4)), dma((2, 4)), dma((2,)),
        ],
        compiler_params=pltpu.CompilerParams(collective_id=0, has_side_effects=True, vmem_limit_bytes=40 * 1024 * 1024),
    )(*(pltpu.with_memory_space_constraint(a, pltpu.HBM) for a in args))
    one = (
        shape((16, 256), f32), shape((16, 256), f32), shape((2048, 256), bf16), shape((2, 256), f32), shape((2, 256), f32),
    )
    return pl.pallas_call(
        update_kernel,
        out_shape=one + one,
        in_specs=[vmem] * 6,
        out_specs=(hbm,) * 10,
        scratch_shapes=[
            room((2, 8, 256, 256), bf16), room((2, 2, 16, 256), f32), room((2, 2, 2, 256), f32), dma((2, 8)), dma((2, 4)),
        ],
        compiler_params=pltpu.CompilerParams(vmem_limit_bytes=40 * 1024 * 1024),
    )(*mid)


def solution(mesh):
    split = Mesh(mesh.devices.reshape(8, 8, 2, mesh.shape["tp"]), ("z", "y", "c", "tp"))
    rows, tiles = P(FS, None), P(FS, "tp")
    one = (tiles, tiles, P(None, "tp"), tiles, tiles)
    return jax.shard_map(
        body,
        mesh=split,
        in_specs=(rows, tiles, tiles, rows, rows, tiles, tiles, tiles, tiles, tiles, tiles),
        out_specs=one + one,
        check_vma=False,
    )
```

time: 60 us -> 56.3 us (0.938)
  Pallas kernels: 59.2 us -> 55.5 us
    pallas_call x2, Pallas kernels: 59.2 us -> 55.5 us  [the longest x1 53.3 us: body(): pl.pallas_call(exchange_kernel, out_shape=(room((4, 2, 8, 8, 16, 128), bf...]
where the time goes in v4:
time: 56.3 us; the launch traced here: 56.2 us
  Pallas kernels  55.5 us (99%)
  between operations  0.65 us (1%)
    pallas_call x1, Pallas kernels, body(): pl.pallas_call(exchange_kernel, out_shape=(room((4, 2, 8, 8, 16, 128), bf...  53.3 us
    pallas_call x1, Pallas kernels, body(): pl.pallas_call(update_kernel, out_shape=one + one, in_specs=[vmem] * 6, o...  2.24 us

profile of v4, /device:TPU:1, one launch (start us, length us, event | category | flops | bytes accessed | tf_op | source)
XLA Modules:
  0.0 56.2 jit_solution(4333335959697279873)
XLA Ops:
  0.6 53.3 %shard_map.186 = (bf16[4,2,8,8,16,128]{5,4,3,2,1,0:T(8,128)(2,1)S(1)}, f32[8,4,2,2,16,256]{5,4,3,2,1,0:T(8,128)S(1)}, f32[4,2,8,2,16,256]{5,4,3,2,1,0:T(8,128)S(...) custom-call(bf16[192,2048]{1,0:T(8,128)(2,1)} %x_hbm.1, ...), custom_call_target="tpu_custom_call" | custom-call | tf_op jit(solution)/shard_map/pallas_call | solution.py:348
  53.9 2.2 %shard_map.187 = (f32[16,256]{1,0:T(8,128)}, f32[16,256]{1,0:T(8,128)}, bf16[2048,256]{1,0:T(8,128)(2,1)}, f32[2,256]{1,0:T(2,128)}, f32[2,256]{1,0:T(2,128)}, /...) custom-call(bf16[4,2,8,8,16,128]{5,4,3,2,1,0:T(8,128)(2,1)S(1)} %get, ...), custom_call_target="tpu_custom_call" | custom-call | tf_op jit(solution)/shard_map/pallas_call | solution.py:369

commit v5 on v4

--- a/solution.py
+++ b/solution.py
@@ -10,7 +10,6 @@
 FS = ("z", "y", "c")
 N = 8
 FAR_FIRST = (4, 3, 5, 2, 6, 1, 7)
-NEAR_FIRST = (1, 7, 2, 6, 3, 5, 4)
 
 beta_one = 0.9
 beta_two = 0.99
@@ -71,7 +70,7 @@
     x_hbm, cq_hbm, ck_hbm, fq_hbm, fk_hbm, q1_hbm, q2_hbm, k1_hbm, k2_hbm, wq_hbm, wk_hbm,
     FULL, WQ, WK, DD, total_ref, mom_ref,
     xv, cots, CA, fown, MOM, MF, PB, PR, SB, R1, S1, R2, TS, T, M8,
-    loc, out, inn, r2, w1, wr, wl, wd,
+    loc, out, inn, fx, r2, c1, w1, wr, wl, wd,
 ):
     pos = {a: lax.axis_index(a) for a in FS}
     x = lax.axis_index("tp")
@@ -82,7 +81,7 @@
     first_is_y = c == 0
     f, s = jnp.where(first_is_y, y, z), jnp.where(first_is_y, z, y)
     proj, side = x // 2, x % 2
-    D1, DDUP, MS, CS, PS, B1, B2, C1, CD, TSUM, FX, FD = range(12)
+    D1, DDUP, MS, CS, PS, B1, B2, CD, TSUM, FD = range(10)
 
     def on_first(d):
         return {"y": jnp.where(first_is_y, ring(y, d), y), "z": jnp.where(first_is_y, z, ring(z, d))}
@@ -191,11 +190,11 @@
                 same(p.strip(W[k], ring(p.s, 4), c), 7, wd.at[k], other)
 
     weights_step(0)
-    for d in NEAR_FIRST:
+    for d in FAR_FIRST:
         arrived(FULL.at[0, 0, 0], r2.at[d])
         same(FULL.at[x, c, ring(s, -d)], 2, inn.at[DDUP], other)
-    for d in (2, 1, 3):
-        same(FULL.at[x, c], 14, inn.at[FX], {"tp": plane(d)})
+    for d in (1, 3):
+        same(FULL.at[x, c], 14, fx.at[d], {"tp": plane(d)})
 
     arrived(xv, loc.at[5])
     arrived(CA.at[0], loc.at[2])
@@ -229,9 +228,10 @@
                 send(S1.at[plane(e)], R2.at[x * N + s], 10, inn.at[B2], {**on_second(d), "tp": plane(e)})
     R2[x * N + s] = S1[x]
     weights_step(3)
-    arrived(FULL.at[pl.ds(0, 3), 0], inn.at[FX])
-    for d in (1, 2, 3):
-        same(FULL.at[plane(d), c], 15, inn.at[FD], other)
+    for d, h in ((1, 0), (3, 1)):
+        arrived(FULL.at[0, 0], fx.at[d])
+        same(FULL.at[plane(4 - d), c, pl.ds(4 * h, 4)], 16, fx.at[0], {"tp": plane(d)})
+        same(FULL.at[plane(4 - d), c], 15, inn.at[FD], other)
     arrived(MOM.at[pl.ds(0, 7)], inn.at[MS])
     for k in (0, 1):
         for m in (0, 1):
@@ -256,7 +256,8 @@
             T[k, 1, h] = second_new
         sums.append(jnp.sum(squares, axis=(0, 1), keepdims=True))
     for d in FAR_FIRST:
-        same(DD.at[c, f], 11, inn.at[C1], on_first(d))
+        same(DD.at[c, f], 11, c1.at[d], on_first(d))
+    same(DD.at[c, f], 12, inn.at[CD], other)
 
     row = lax.broadcasted_iota(jnp.int32, (2, 128), 0)
     mine = (c * N + f) * 4 + x
@@ -272,8 +273,11 @@
             for b in range(N):
                 M8[k, m, b] = T[k, m, b // 4, 2 * (b % 4) : 2 * (b % 4) + 2, :]
             mom_ref[k, m] = M8[k, m, s]
-    arrived(DD.at[0, pl.ds(0, 7)], inn.at[C1])
-    same(DD.at[c], 12, inn.at[CD], other)
+    for d in FAR_FIRST:
+        arrived(DD.at[0, 0], c1.at[d])
+        same(DD.at[c, ring(f, -d)], 12, inn.at[CD], other)
+    arrived(FULL.at[0, 0], fx.at[0])
+    same(FULL.at[plane(2), c], 15, inn.at[FD], other)
     arrived(TS.at[pl.ds(0, 63)], inn.at[TSUM])
     total = TS[0]
     for b in range(1, 64):
@@ -289,7 +293,7 @@
         FULL.at[0, 0, 0, pl.ds(0, 7)], FULL.at[0, 0, pl.ds(0, 7)], FULL.at[0, 0], MOM.at[pl.ds(0, 7)],
         CA.at[pl.ds(0, 3)], WQ.at[pl.ds(0, 7), 0, :, 0], WQ.at[pl.ds(0, 7)], WQ, PB.at[0], R1.at[pl.ds(0, 7)],
         R2.at[pl.ds(0, 31)], DD.at[0, pl.ds(0, 7)], DD.at[0], TS.at[pl.ds(0, 63)],
-        FULL.at[pl.ds(0, 3), 0], FULL.at[pl.ds(0, 3), 0],
+        FULL.at[pl.ds(0, 2), 0], FULL.at[pl.ds(0, 3), 0], FULL.at[0, 0],
     )):
         arrived(view, out.at[group])
 
@@ -359,7 +363,7 @@
             room((2, 8, 4, 8, 256), f32), room((8, 4, 8, 256), f32), room((8, 4, 8, 256), f32), room((8, 4, 8, 256), f32),
             room((4, 8, 256), f32), room((32, 8, 256), f32), room((64, 2, 128), f32),
             room((2, 2, 2, 8, 256), f32), room((2, 2, 8, 2, 256), f32),
-            dma((6,)), dma((16,)), dma((12,)), dma((8,)), dma((2,)), dma((2, 4)), dma((2, 4)), dma((2,)),
+            dma((6,)), dma((17,)), dma((10,)), dma((4,)), dma((8,)), dma((8,)), dma((2,)), dma((2, 4)), dma((2, 4)), dma((2,)),
         ],
         compiler_params=pltpu.CompilerParams(collective_id=0, has_side_effects=True, vmem_limit_bytes=40 * 1024 * 1024),
     )(*(pltpu.with_memory_space_constraint(a, pltpu.HBM) for a in args))

time: 56.3 us -> 56.8 us (level)
  no operation moved by 1% of the time
where the time goes in v5:
time: 56.8 us; the launch traced here: 56.6 us
  Pallas kernels  55.9 us (98%)
  between operations  0.65 us (1%)
    pallas_call x1, Pallas kernels, body(): pl.pallas_call(exchange_kernel, out_shape=(room((4, 2, 8, 8, 16, 128), bf...  53.7 us
    pallas_call x1, Pallas kernels, body(): pl.pallas_call(update_kernel, out_shape=one + one, in_specs=[vmem] * 6, o...  2.24 us

profile of v5, /device:TPU:1, one launch (start us, length us, event | category | flops | bytes accessed | tf_op | source)
XLA Modules:
  0.0 56.6 jit_solution(13032863850825280600)
XLA Ops:
  0.6 53.7 %shard_map.186 = (bf16[4,2,8,8,16,128]{5,4,3,2,1,0:T(8,128)(2,1)S(1)}, f32[8,4,2,2,16,256]{5,4,3,2,1,0:T(8,128)S(1)}, f32[4,2,8,2,16,256]{5,4,3,2,1,0:T(8,128)S(...) custom-call(bf16[192,2048]{1,0:T(8,128)(2,1)} %x_hbm.1, ...), custom_call_target="tpu_custom_call" | custom-call | tf_op jit(solution)/shard_map/pallas_call | solution.py:352
  54.4 2.2 %shard_map.187 = (f32[16,256]{1,0:T(8,128)}, f32[16,256]{1,0:T(8,128)}, bf16[2048,256]{1,0:T(8,128)(2,1)}, f32[2,256]{1,0:T(2,128)}, f32[2,256]{1,0:T(2,128)}, /...) custom-call(bf16[4,2,8,8,16,128]{5,4,3,2,1,0:T(8,128)(2,1)S(1)} %get, ...), custom_call_target="tpu_custom_call" | custom-call | tf_op jit(solution)/shard_map/pallas_call | solution.py:373
